TPU v7x, 32 devices: a whole 2x2x4 slice. The times are simulated.
32 devices in a mesh: grp: 2 (over y), dp: 2 (over x), kv: 4 (over z), tp: 2 (over core).
Axes of the slice: x: 2, y: 2, z: 4, core: 2. Of those that a mesh axis runs over, the one named last changes fastest.
Arguments:
- tokens: bfloat16 [32, 2048], P(('grp', 'dp'), ('kv', 'tp')), parts along dimension 0, may hold values from -40 to 40
- past_state: float32 [32, 16, 128, 128], P(('grp', 'dp', 'kv'), 'tp'), parts along dimension 0, may hold values from -4 to 4
- mix_gain: float32 [2048], P('kv'), may hold values from 0.1 to 1.9
- w_query: bfloat16 [2048, 2048], P('kv', 'tp'), may hold values from -0.125 to 0.125
- w_forget: bfloat16 [2048, 2048], P('kv', 'tp'), may hold values from -0.125 to 0.125
- w_value: bfloat16 [2048, 2048], P('kv', 'tp'), may hold values from -0.125 to 0.125
- w_gate_out: bfloat16 [2048, 2048], P('kv', 'tp'), may hold values from -0.125 to 0.125
- floor_logits: float32 [2048], P('tp'), may hold values from -6 to 6
- head_gain: float32 [128], replicated, may hold values from 0.1 to 1.9
- w_out: bfloat16 [2048, 2048], P(None, ('kv', 'tp')), may hold values from -0.125 to 0.125
- mlp_gain: float32 [2048], replicated, may hold values from 0.1 to 1.9
- w_gate: bfloat16 [2048, 5632], P(None, ('kv', 'tp')), may hold values from -0.125 to 0.125
- w_up: bfloat16 [2048, 5632], P(None, ('kv', 'tp')), may hold values from -0.125 to 0.125
- w_down: bfloat16 [5632, 2048], P(('kv', 'tp')), may hold values from -0.109375 to 0.109375
Outputs:
- result: bfloat16 [32, 2048], P(('grp', 'dp'), ('kv', 'tp')), parts along dimension 0
- new_state: float32 [32, 16, 128, 128], P(('grp', 'dp', 'kv'), 'tp'), parts along dimension 0
There are 2 independent parts, one for each index of `grp`. A program takes and returns all parts, laid end to end along the dimension named above; an argument that names none is the same for every part. Nothing has to cross between parts.
All inputs are finite; a program needn't handle non-finite values.
Results may differ from a plain program's by a relative error of at most 0.0091.
Values may be sent and summed in bfloat16 or wider, within the bound.
A program may use at most 64 MiB of HBM per device.

v0:
```python
import functools

import jax
import jax.numpy as jnp
from jax import lax
from jax.experimental import pallas as pl
from jax.experimental.pallas import tpu as pltpu
from jax.sharding import PartitionSpec as P

epsilon = 1e-06
F32 = jnp.float32
BF16 = jnp.bfloat16
MESH = pl.DeviceIdType.MESH


def sigmoid(a):
    return 1.0 / (1.0 + jnp.exp(-a))


def silu(a):
    return a / (1.0 + jnp.exp(-a))


def dot_t(a, b):
    return lax.dot_general(a, b, (((1,), (1,)), ((), ())), preferred_element_type=F32)


def kernel(
    K,
    T,
    tokens,
    past,
    mix_gain,
    w_query,
    w_forget,
    w_value,
    w_gate_out,
    floor_logits,
    head_gain,
    w_out,
    mlp_gain,
    w_gate,
    w_up,
    w_down,
    result,
    new_state,
    tok_v,
    past_v,
    mixg_v,
    proj_v,
    floor_v,
    hgain_v,
    wout_v,
    mlpg_v,
    wgate_v,
    wup_v,
    wdown_v,
    sq_send,
    sq_recv,
    part,
    part_send,
    part_recv,
    head_v,
    mix_all,
    mix_f,
    mid_all,
    term_send,
    term_recv,
    local_sem,
    tok_ss,
    tok_rs,
    sq_ss,
    sq_rs,
    part_ss,
    part_rs,
    mix_ss,
    mix_rs,
    mid_ss,
    mid_rs,
    term_ss,
    term_rs,
):
    R, W = tokens.shape
    RL, H, DK, DV = past.shape
    D = w_gate.shape[1]
    kv = lax.axis_index("kv")
    tp = lax.axis_index("tp")
    me = kv * T + tp

    def far(k):
        return min(k, K - k)

    hops = sorted(range(1, K), key=far)
    near = [(0, dt) for dt in range(1, T)] + [(dk, dt) for dk in hops for dt in range(T)]

    def other(dk, dt):
        return lax.rem(kv + dk, K), lax.rem(tp + dt, T)

    def source(dk, dt):
        return lax.rem(kv + K - dk, K), lax.rem(tp + T - dt, T)

    def load(i, src, dst):
        copy = pltpu.make_async_copy(src, dst, local_sem.at[i])
        copy.start()
        return copy

    c_tok = load(0, tokens, tok_v.at[tp])
    c_mixg = load(1, mix_gain, mixg_v)
    c_proj = [
        load(2 + i, w, proj_v.at[i])
        for i, w in enumerate((w_forget, w_query, w_value, w_gate_out))
    ]
    c_past = load(6, past, past_v)
    c_floor = load(7, floor_logits, floor_v)
    c_hgain = load(8, head_gain, hgain_v)
    c_mlpg = load(9, mlp_gain, mlpg_v)
    c_wout = load(10, w_out, wout_v)
    c_wgate = load(11, w_gate, wgate_v)
    c_wup = load(12, w_up, wup_v)
    c_wdown = load(13, w_down, wdown_v)

    barrier = pltpu.get_barrier_semaphore()
    for dk, dt in near:
        k, t = other(dk, dt)
        pl.semaphore_signal(barrier, inc=1, device_id={"kv": k, "tp": t}, device_id_type=MESH)
    c_tok.wait()
    pl.semaphore_wait(barrier, len(near))

    def send(src, dst, ss, rs, k, t):
        copy = pltpu.make_async_remote_copy(
            src_ref=src,
            dst_ref=dst,
            send_sem=ss,
            recv_sem=rs,
            device_id={"kv": k, "tp": t},
            device_id_type=MESH,
        )
        copy.start()
        return copy

    def arrived(dst, ss, rs):
        pltpu.make_async_remote_copy(
            src_ref=dst,
            dst_ref=dst,
            send_sem=ss,
            recv_sem=rs,
            device_id={"kv": kv, "tp": lax.rem(tp + 1, T)},
            device_id_type=MESH,
        ).wait_recv()

    sent = []
    for dt in range(1, T):
        k, t = other(0, dt)
        sent.append(send(tok_v.at[tp], tok_v.at[tp], tok_ss.at[dt], tok_rs.at[tp], k, t))

    c_mixg.wait()
    gained = []
    early = []
    square = jnp.zeros((R, 1), F32)
    for dt in range(T):
        t = lax.rem(tp + T - dt, T)
        if dt:
            arrived(tok_v.at[t], tok_ss.at[0], tok_rs.at[t])
        block = tok_v[t].astype(F32)
        square = square + jnp.sum(block * block, axis=1, keepdims=True)
        gained.append((block * mixg_v[t]).astype(BF16))
        if dt == 0:
            rows = pl.ds(pl.multiple_of(t * W, W), W)
            for i in range(4):
                c_proj[i].wait()
                early.append(
                    jnp.dot(gained[0], proj_v[i, rows, :], preferred_element_type=F32)
                )
    square = jnp.broadcast_to(square, (R, DK))
    for h in range(H):
        sq_send[:, h, :] = square
    for dk in hops[::-1]:
        k, t = other(dk, 0)
        sent.append(
            send(sq_send.at[pl.ds(k * RL, RL)], sq_recv.at[kv], sq_ss.at[dk], sq_rs.at[kv], k, t)
        )
    for i in range(4):
        total = early[i]
        for dt in range(1, T):
            t = lax.rem(tp + T - dt, T)
            rows = pl.ds(pl.multiple_of(t * W, W), W)
            piece = jnp.dot(gained[dt], proj_v[i, rows, :], preferred_element_type=F32)
            total = total + piece
        for h in range(H):
            part[i, :, h, :] = total[:, h * DK : (h + 1) * DK]
        for k in range(K):
            part_send[i, k] = part[i, k * RL : (k + 1) * RL].reshape(RL * H, DK).astype(BF16)
        for dk in hops[::-1]:
            k, t = other(dk, 0)
            sent.append(
                send(
                    part_send.at[i, k],
                    part_recv.at[i, kv],
                    part_ss.at[i, dk],
                    part_rs.at[i, kv],
                    k,
                    t,
                )
            )

    c_floor.wait()
    c_hgain.wait()
    square = sq_send[pl.ds(kv * RL, RL)].reshape(RL * H, DK)
    for dk in hops:
        k, t = source(dk, 0)
        arrived(sq_recv.at[k], sq_ss.at[dk], sq_rs.at[k])
        square = square + sq_recv[k].reshape(RL * H, DK)
    row_scale = lax.rsqrt(square / D + epsilon)

    def summed(i):
        total = part[i, pl.ds(kv * RL, RL)].reshape(RL * H, DK)
        for dk in hops:
            k, t = source(dk, 0)
            arrived(part_recv.at[i, k], part_ss.at[i, dk], part_rs.at[i, k])
            total = total + part_recv[i, k].astype(F32)
        return total * row_scale

    lower = sigmoid(floor_v[...])
    lower = jnp.concatenate([lower] * RL, axis=0)
    forget = lower + (1.0 - lower) * sigmoid(summed(0))
    activ = silu(summed(1))
    columns = jnp.concatenate([forget, activ], axis=0).T
    value = summed(2)
    c_past.wait()
    for s in range(RL):
        for h in range(H):
            i = s * H + h
            row = value[i : i + 1, :]
            f_col = columns[:, i : i + 1]
            q_col = columns[:, RL * H + i : RL * H + i + 1]
            new = row + f_col * (past_v[s, h] - row)
            new_state[s, h] = new
            head_v[i : i + 1, :] = jnp.sum(new * q_col, axis=0, keepdims=True)
    head_out = head_v[...]
    normed = head_out * lax.rsqrt(
        jnp.mean(head_out * head_out, axis=1, keepdims=True) + epsilon
    )
    mixed = normed * hgain_v[...] * silu(summed(3))
    mix_all[tp, kv] = mixed.astype(BF16)
    for dk, dt in near[::-1]:
        k, t = other(dk, dt)
        slot = mix_all.at[tp, kv]
        sent.append(send(slot, slot, mix_ss.at[dk, dt], mix_rs.at[kv, tp], k, t))

    def spread(t, k):
        mix_f[t, pl.ds(k * RL, RL)] = mix_all[t, k].astype(F32).reshape(RL, H, DV)

    spread(tp, kv)
    for dk, dt in near:
        k, t = source(dk, dt)
        arrived(mix_all.at[t, k], mix_ss.at[dk, dt], mix_rs.at[k, t])
        spread(t, k)
    every_head = jnp.concatenate(
        [mix_f[t, :, h, :].astype(BF16) for t in range(T) for h in range(H)], axis=1
    )
    c_wout.wait()
    middle = tok_v[tp].astype(F32) + jnp.dot(
        every_head, wout_v[...], preferred_element_type=F32
    )
    middle = middle.astype(BF16)
    mid_all[me] = middle
    for dk, dt in near[::-1]:
        k, t = other(dk, dt)
        slot = mid_all.at[me]
        sent.append(send(slot, slot, mid_ss.at[dk, dt], mid_rs.at[kv, tp], k, t))

    c_mlpg.wait()
    square = jnp.zeros((R, 1), F32)
    gate = None
    if W % 128 == 0:
        groups = [[peer] for peer in [(0, 0)] + near]
    else:
        groups = [[(dk, dt) for dt in range(T)] for dk in [0] + hops]
    for group in groups:
        for dk, dt in group:
            k, t = source(dk, dt)
            if dk or dt:
                arrived(mid_all.at[k * T + t], mid_ss.at[dk, dt], mid_rs.at[k, t])
        k, t = source(*group[0])
        j = k * T + (t if len(group) == 1 else 0)
        blocks = []
        for i in range(len(group)):
            block = mid_all[j + i].astype(F32)
            square = square + jnp.sum(block * block, axis=1, keepdims=True)
            blocks.append((block * mlpg_v[j + i]).astype(BF16))
        block = jnp.concatenate(blocks, axis=1) if len(blocks) > 1 else blocks[0]
        width = len(group) * W
        lanes = pl.ds(pl.multiple_of(j * W, width), width)
        if gate is None:
            c_wgate.wait()
        g = dot_t(block, wgate_v[:, lanes])
        if gate is None:
            c_wup.wait()
        u = dot_t(block, wup_v[:, lanes])
        gate, upward = (g, u) if gate is None else (gate + g, upward + u)
    mlp_scale = lax.rsqrt(square / D + epsilon)
    hidden = (silu(gate * mlp_scale) * (upward * mlp_scale)).astype(BF16)
    c_wdown.wait()
    for dk in hops[::-1] + [0]:
        k, _ = other(dk, 0)
        lanes = pl.ds(pl.multiple_of(k * T * W, T * W), T * W)
        chunk = jnp.dot(hidden, wdown_v[:, lanes], preferred_element_type=F32).astype(BF16)
        for t in range(T):
            term_send[k * T + t] = chunk[:, t * W : (t + 1) * W]
        for dt in range(0 if dk else 1, T):
            _, t = other(dk, dt)
            sent.append(
                send(
                    term_send.at[k * T + t],
                    term_recv.at[me],
                    term_ss.at[dk, dt],
                    term_rs.at[kv, tp],
                    k,
                    t,
                )
            )
    total = term_send[me].astype(F32)
    for dk, dt in near:
        k, t = source(dk, dt)
        j = k * T + t
        arrived(term_recv.at[j], term_ss.at[dk, dt], term_rs.at[k, t])
        total = total + term_recv[j].astype(F32)
    result[...] = (middle.astype(F32) + total).astype(BF16)
    for copy in sent:
        copy.wait_send()


def body(
    tokens,
    past_state,
    mix_gain,
    w_query,
    w_forget,
    w_value,
    w_gate_out,
    floor_logits,
    head_gain,
    w_out,
    mlp_gain,
    w_gate,
    w_up,
    w_down,
):
    K = lax.axis_size("kv")
    T = lax.axis_size("tp")
    n = K * T
    R, W = tokens.shape
    RL, H, DK, DV = past_state.shape
    args = (
        tokens,
        past_state,
        mix_gain.reshape(T, 1, W),
        w_query,
        w_forget,
        w_value,
        w_gate_out,
        floor_logits.reshape(H, DK),
        head_gain.reshape(1, DV),
        w_out,
        mlp_gain.reshape(n, 1, W),
        w_gate.T,
        w_up.T,
        w_down,
    )
    V = pltpu.VMEM
    dma = pltpu.SemaphoreType.DMA
    anywhere = pl.BlockSpec(memory_space=pl.ANY)
    return pl.pallas_call(
        functools.partial(kernel, K, T),
        out_shape=(
            pltpu.VMEM((R, W), BF16),
            pltpu.VMEM(past_state.shape, F32),
        ),
        in_specs=[anywhere] * len(args),
        out_specs=(pl.BlockSpec(memory_space=pltpu.VMEM),)*2,
        scratch_shapes=[
            V((T, R, W), BF16),
            V(past_state.shape, F32),
            V((T, 1, W), F32),
            V((4,) + w_query.shape, BF16),
            V((H, DK), F32),
            V((1, DV), F32),
            V(w_out.shape, BF16),
            V((n, 1, W), F32),
            V(w_gate.shape[::-1], BF16),
            V(w_up.shape[::-1], BF16),
            V(w_down.shape, BF16),
            V((R, H, DK), F32),
            V((K, RL, H, DK), F32),
            V((4, R, H, DK), F32),
            V((4, K, RL * H, DK), BF16),
            V((4, K, RL * H, DK), BF16),
            V((RL * H, DV), F32),
            V((T, K, RL * H, DV), BF16),
            V((T, R, H, DV), F32),
            V((n, R, W), BF16),
            V((n, R, W), BF16),
            V((n, R, W), BF16),
            dma((14,)),
            dma((T,)),
            dma((T,)),
            dma((K,)),
            dma((K,)),
            dma((4, K)),
            dma((4, K)),
            dma((K, T)),
            dma((K, T)),
            dma((K, T)),
            dma((K, T)),
            dma((K, T)),
            dma((K, T)),
        ],
        compiler_params=pltpu.CompilerParams(
            collective_id=0, has_side_effects=True, vmem_limit_bytes=60 * 1024 * 1024
        ),
    )(*args)


def solution(mesh):
    placed = (
        P(("grp", "dp"), ("kv", "tp")),
        P(("grp", "dp", "kv"), "tp", None, None),
        P("kv"),
        P("kv", "tp"),
        P("kv", "tp"),
        P("kv", "tp"),
        P("kv", "tp"),
        P("tp"),
        P(),
        P(None, ("kv", "tp")),
        P(),
        P(None, ("kv", "tp")),
        P(None, ("kv", "tp")),
        P(("kv", "tp"), None),
    )
    return jax.shard_map(
        body,
        mesh=mesh,
        in_specs=placed,
        out_specs=(P(("grp", "dp"), ("kv", "tp")), P(("grp", "dp", "kv"), "tp", None, None)),
        check_vma=False,
    )
```

profile of v0, /device:TPU:0, one launch (start us, length us, event | category | flops | bytes accessed | tf_op | source)
XLA Modules:
  0.0 27.3 jit_solution(8585143105486297976)
XLA Ops:
  0.6 25.1 %shard_map.149 = (bf16[8,256]{1,0:T(8,128)(2,1)S(1)}, f32[2,8,128,128]{3,2,1,0:T(8,128)S(1)}) custom-call(bf16[8,256]{1,0:T(8,128)(2,1)} %tokens.1, f32[2,8,128,128]{3,2,1,0:T(8,128)} %past.1, f32[2,1,256]{2,1,0:T(1,128)} %bitcast.10, bf16[512,1024]{1,0:T(8,128)(2,1)} %w_query.1, bf16[512,1024]{1,0:T(8,128)(2,1)} %w_forget.1, bf16[512,1024]{1,0:T(8,128)(2,1)} %w_value.1, ...), custom_call_target="tpu_custom_call" | custom-call | tf_op jit(solution)/shard_map/pallas_call | solution.py:373
  25.8 0.6 %copy.18 = bf16[8,256]{1,0:T(8,128)(2,1)} copy(bf16[8,256]{1,0:T(8,128)(2,1)S(1)} %get-tuple-element.2) | data formatting | bytes 8192
  26.4 1.0 %copy.19 = f32[2,8,128,128]{3,2,1,0:T(8,128)} copy(f32[2,8,128,128]{3,2,1,0:T(8,128)S(1)} %get-tuple-element.3) | data formatting | bytes 2097152
where the time goes:
time: 27.5 us; the launch traced here: 27.3 us
  Pallas kernels  25.1 us (91%)
  local copies, waits for them, and re-layouts  1.56 us (6%)
  between operations  0.64 us (2%)
    pallas_call x1, Pallas kernels, body(): pl.pallas_call(functools.partial(kernel, K, T), out_shape=(pltpu.VMEM((R,...  25.1 us
    unnamed x2, local copies, waits for them, and re-layouts  1.56 us

commit v1 on v0

--- a/solution.py
+++ b/solution.py
@@ -60,7 +60,7 @@
     part,
     part_send,
     part_recv,
-    head_v,
+    split_v,
     mix_all,
     mix_f,
     mid_all,
@@ -87,17 +87,25 @@
     tp = lax.axis_index("tp")
     me = kv * T + tp
 
-    def far(k):
-        return min(k, K - k)
-
-    hops = sorted(range(1, K), key=far)
+    paired = K & (K - 1) == 0
+    hops = list(range(1, K))
     near = [(0, dt) for dt in range(1, T)] + [(dk, dt) for dk in hops for dt in range(T)]
 
+    def flip(k, dk):
+        bit = 1
+        while bit <= dk:
+            if dk & bit:
+                k = k + bit - 2 * bit * lax.rem(k // bit, 2)
+            bit *= 2
+        return k
+
     def other(dk, dt):
-        return lax.rem(kv + dk, K), lax.rem(tp + dt, T)
+        k = flip(kv, dk) if paired else lax.rem(kv + dk, K)
+        return k, (lax.rem(tp + dt, T) if dk == 0 else dt)
 
     def source(dk, dt):
-        return lax.rem(kv + K - dk, K), lax.rem(tp + T - dt, T)
+        k = flip(kv, dk) if paired else lax.rem(kv + K - dk, K)
+        return k, (lax.rem(tp + T - dt, T) if dk == 0 else T - 1 - dt)
 
     def load(i, src, dst):
         copy = pltpu.make_async_copy(src, dst, local_sem.at[i])
@@ -172,12 +180,12 @@
                     jnp.dot(gained[0], proj_v[i, rows, :], preferred_element_type=F32)
                 )
     square = jnp.broadcast_to(square, (R, DK))
-    for h in range(H):
-        sq_send[:, h, :] = square
+    for k in range(K):
+        sq_send[k] = square[k * RL : (k + 1) * RL]
     for dk in hops[::-1]:
-        k, t = other(dk, 0)
+        k, t = other(dk, 0)[0], tp
         sent.append(
-            send(sq_send.at[pl.ds(k * RL, RL)], sq_recv.at[kv], sq_ss.at[dk], sq_rs.at[kv], k, t)
+            send(sq_send.at[k], sq_recv.at[kv], sq_ss.at[dk], sq_rs.at[kv], k, t)
         )
     for i in range(4):
         total = early[i]
@@ -191,7 +199,7 @@
         for k in range(K):
             part_send[i, k] = part[i, k * RL : (k + 1) * RL].reshape(RL * H, DK).astype(BF16)
         for dk in hops[::-1]:
-            k, t = other(dk, 0)
+            k, t = other(dk, 0)[0], tp
             sent.append(
                 send(
                     part_send.at[i, k],
@@ -205,12 +213,25 @@
 
     c_floor.wait()
     c_hgain.wait()
-    square = sq_send[pl.ds(kv * RL, RL)].reshape(RL * H, DK)
+    lower = sigmoid(floor_v[...])
+    lower = jnp.concatenate([lower] * RL, axis=0)
+    c_past.wait()
+    for s in range(RL):
+        for h in range(H):
+            rows = pl.ds((s * H + h) * DK, DK)
+            block = past_v[s, h]
+            high = block.astype(BF16)
+            split_v[rows, :DV] = high
+            split_v[rows, DV:] = (block - high.astype(F32)).astype(BF16)
+    square = sq_send[kv]
     for dk in hops:
         k, t = source(dk, 0)
         arrived(sq_recv.at[k], sq_ss.at[dk], sq_rs.at[k])
-        square = square + sq_recv[k].reshape(RL * H, DK)
+        square = square + sq_recv[k]
     row_scale = lax.rsqrt(square / D + epsilon)
+    row_scale = jnp.concatenate(
+        [jnp.broadcast_to(row_scale[s : s + 1], (H, DK)) for s in range(RL)], axis=0
+    )
 
     def summed(i):
         total = part[i, pl.ds(kv * RL, RL)].reshape(RL * H, DK)
@@ -220,23 +241,20 @@
             total = total + part_recv[i, k].astype(F32)
         return total * row_scale
 
-    lower = sigmoid(floor_v[...])
-    lower = jnp.concatenate([lower] * RL, axis=0)
     forget = lower + (1.0 - lower) * sigmoid(summed(0))
     activ = silu(summed(1))
-    columns = jnp.concatenate([forget, activ], axis=0).T
+    weight = activ * forget
+    high = weight.astype(BF16).astype(F32)
+    weight = jnp.concatenate([high, weight - high], axis=0)
+    owner = lax.rem(lax.broadcasted_iota(jnp.int32, weight.shape, 0), RL * H)
+    left = jnp.concatenate(
+        [jnp.where(owner == i, weight, 0.0).astype(BF16) for i in range(RL * H)], axis=1
+    )
+    wide = jnp.dot(left, split_v[...], preferred_element_type=F32)
+    head_out = wide[: RL * H, :DV] + (wide[: RL * H, DV:] + wide[RL * H :, :DV])
+    rest = jnp.sum(activ * (1.0 - forget), axis=1, keepdims=True)
     value = summed(2)
-    c_past.wait()
-    for s in range(RL):
-        for h in range(H):
-            i = s * H + h
-            row = value[i : i + 1, :]
-            f_col = columns[:, i : i + 1]
-            q_col = columns[:, RL * H + i : RL * H + i + 1]
-            new = row + f_col * (past_v[s, h] - row)
-            new_state[s, h] = new
-            head_v[i : i + 1, :] = jnp.sum(new * q_col, axis=0, keepdims=True)
-    head_out = head_v[...]
+    head_out = head_out + value * rest
     normed = head_out * lax.rsqrt(
         jnp.mean(head_out * head_out, axis=1, keepdims=True) + epsilon
     )
@@ -246,6 +264,13 @@
         k, t = other(dk, dt)
         slot = mix_all.at[tp, kv]
         sent.append(send(slot, slot, mix_ss.at[dk, dt], mix_rs.at[kv, tp], k, t))
+
+    columns = forget.T
+    for s in range(RL):
+        for h in range(H):
+            i = s * H + h
+            row = value[i : i + 1, :]
+            new_state[s, h] = row + columns[:, i : i + 1] * (past_v[s, h] - row)
 
     def spread(t, k):
         mix_f[t, pl.ds(k * RL, RL)] = mix_all[t, k].astype(F32).reshape(RL, H, DV)
@@ -390,12 +415,12 @@
             V(w_gate.shape[::-1], BF16),
             V(w_up.shape[::-1], BF16),
             V(w_down.shape, BF16),
-            V((R, H, DK), F32),
-            V((K, RL, H, DK), F32),
+            V((K, RL, DK), F32),
+            V((K, RL, DK), F32),
             V((4, R, H, DK), F32),
             V((4, K, RL * H, DK), BF16),
             V((4, K, RL * H, DK), BF16),
-            V((RL * H, DV), F32),
+            V((RL * H * DK, 2 * DV), BF16),
             V((T, K, RL * H, DV), BF16),
             V((T, R, H, DV), F32),
             V((n, R, W), BF16),

time: 27.5 us -> 25.7 us (0.935)
  Pallas kernels: 25.1 us -> 23.3 us
    pallas_call x1, Pallas kernels: 25.1 us -> 23.3 us  [body(): pl.pallas_call(functools.partial(kernel, K, T), out_shape=(pltpu.VMEM((R,...]
where the time goes in v1:
time: 25.7 us; the launch traced here: 25.5 us
  Pallas kernels  23.3 us (91%)
  local copies, waits for them, and re-layouts  1.56 us (6%)
  between operations  0.64 us (2%)
    pallas_call x1, Pallas kernels, body(): pl.pallas_call(functools.partial(kernel, K, T), out_shape=(pltpu.VMEM((R,...  23.3 us
    unnamed x2, local copies, waits for them, and re-layouts  1.56 us

profile of v1, /device:TPU:0, one launch (start us, length us, event | category | flops | bytes accessed | tf_op | source)
XLA Modules:
  0.0 25.5 jit_solution(9667419196769885095)
XLA Ops:
  0.6 23.3 %shard_map.149 = (bf16[8,256]{1,0:T(8,128)(2,1)S(1)}, f32[2,8,128,128]{3,2,1,0:T(8,128)S(1)}) custom-call(bf16[8,256]{1,0:T(8,128)(2,1)} %tokens.1, f32[2,8,128,128]{3,2,1,0:T(8,128)} %past.1, f32[2,1,256]{2,1,0:T(1,128)} %bitcast.10, bf16[512,1024]{1,0:T(8,128)(2,1)} %w_query.1, bf16[512,1024]{1,0:T(8,128)(2,1)} %w_forget.1, bf16[512,1024]{1,0:T(8,128)(2,1)} %w_value.1, ...), custom_call_target="tpu_custom_call" | custom-call | tf_op jit(solution)/shard_map/pallas_call | solution.py:398
  23.9 0.6 %copy.18 = bf16[8,256]{1,0:T(8,128)(2,1)} copy(bf16[8,256]{1,0:T(8,128)(2,1)S(1)} %get-tuple-element.2) | data formatting | bytes 8192
  24.5 1.0 %copy.19 = f32[2,8,128,128]{3,2,1,0:T(8,128)} copy(f32[2,8,128,128]{3,2,1,0:T(8,128)S(1)} %get-tuple-element.3) | data formatting | bytes 2097152

commit v2 on v1

--- a/solution.py
+++ b/solution.py
@@ -87,25 +87,24 @@
     tp = lax.axis_index("tp")
     me = kv * T + tp
 
-    paired = K & (K - 1) == 0
     hops = list(range(1, K))
-    near = [(0, dt) for dt in range(1, T)] + [(dk, dt) for dk in hops for dt in range(T)]
-
-    def flip(k, dk):
-        bit = 1
-        while bit <= dk:
-            if dk & bit:
-                k = k + bit - 2 * bit * lax.rem(k // bit, 2)
-            bit *= 2
-        return k
-
-    def other(dk, dt):
-        k = flip(kv, dk) if paired else lax.rem(kv + dk, K)
-        return k, (lax.rem(tp + dt, T) if dk == 0 else dt)
-
-    def source(dk, dt):
-        k = flip(kv, dk) if paired else lax.rem(kv + K - dk, K)
-        return k, (lax.rem(tp + T - dt, T) if dk == 0 else T - 1 - dt)
+    near = [(0, dt) for dt in range(1, T)] + [(j, dt) for j in hops for dt in range(T)]
+    upper = (2 * kv) // K
+    short = upper * (K - 1 - kv) + (1 - upper) * kv
+    ahead = 1 - 2 * upper
+
+    def hop(j):
+        if j == 0:
+            return kv
+        both = jnp.minimum(jnp.maximum(2 * short - j + 1, 0), 1)
+        step = both * ((j + 1) // 2) * (2 * (j % 2) - 1) + (1 - both) * (j - short)
+        return kv + ahead * step
+
+    def other(j, dt):
+        return hop(j), (lax.rem(tp + dt, T) if j == 0 else dt)
+
+    def source(j, dt):
+        return hop(j), (lax.rem(tp + T - dt, T) if j == 0 else T - 1 - dt)
 
     def load(i, src, dst):
         copy = pltpu.make_async_copy(src, dst, local_sem.at[i])
@@ -122,17 +121,16 @@
     c_floor = load(7, floor_logits, floor_v)
     c_hgain = load(8, head_gain, hgain_v)
     c_mlpg = load(9, mlp_gain, mlpg_v)
-    c_wout = load(10, w_out, wout_v)
-    c_wgate = load(11, w_gate, wgate_v)
-    c_wup = load(12, w_up, wup_v)
-    c_wdown = load(13, w_down, wdown_v)
 
     barrier = pltpu.get_barrier_semaphore()
-    for dk, dt in near:
-        k, t = other(dk, dt)
+
+    def signal(k, t):
         pl.semaphore_signal(barrier, inc=1, device_id={"kv": k, "tp": t}, device_id_type=MESH)
+
+    for j in hops[::-1]:
+        signal(hop(j), 0)
+    signal(kv, 1 - tp)
     c_tok.wait()
-    pl.semaphore_wait(barrier, len(near))
 
     def send(src, dst, ss, rs, k, t):
         copy = pltpu.make_async_remote_copy(
@@ -157,59 +155,88 @@
         ).wait_recv()
 
     sent = []
-    for dt in range(1, T):
-        k, t = other(0, dt)
-        sent.append(send(tok_v.at[tp], tok_v.at[tp], tok_ss.at[dt], tok_rs.at[tp], k, t))
+    swap = pltpu.make_async_remote_copy(
+        src_ref=tok_v.at[tp],
+        dst_ref=tok_v.at[tp],
+        send_sem=tok_ss,
+        recv_sem=tok_rs,
+        device_id={"kv": kv, "tp": 1 - tp},
+        device_id_type=MESH,
+    )
+    sent.append(swap)
+
+    @pl.when(tp == 1)
+    def _():
+        pl.semaphore_wait(barrier, 1)
+        swap.start()
 
     c_mixg.wait()
-    gained = []
-    early = []
-    square = jnp.zeros((R, 1), F32)
-    for dt in range(T):
-        t = lax.rem(tp + T - dt, T)
-        if dt:
-            arrived(tok_v.at[t], tok_ss.at[0], tok_rs.at[t])
+
+    def features(t):
         block = tok_v[t].astype(F32)
-        square = square + jnp.sum(block * block, axis=1, keepdims=True)
-        gained.append((block * mixg_v[t]).astype(BF16))
-        if dt == 0:
-            rows = pl.ds(pl.multiple_of(t * W, W), W)
-            for i in range(4):
-                c_proj[i].wait()
-                early.append(
-                    jnp.dot(gained[0], proj_v[i, rows, :], preferred_element_type=F32)
-                )
-    square = jnp.broadcast_to(square, (R, DK))
-    for k in range(K):
-        sq_send[k] = square[k * RL : (k + 1) * RL]
-    for dk in hops[::-1]:
-        k, t = other(dk, 0)[0], tp
-        sent.append(
-            send(sq_send.at[k], sq_recv.at[kv], sq_ss.at[dk], sq_rs.at[kv], k, t)
-        )
-    for i in range(4):
-        total = early[i]
-        for dt in range(1, T):
-            t = lax.rem(tp + T - dt, T)
-            rows = pl.ds(pl.multiple_of(t * W, W), W)
-            piece = jnp.dot(gained[dt], proj_v[i, rows, :], preferred_element_type=F32)
-            total = total + piece
+        square = jnp.sum(block * block, axis=1, keepdims=True)
+        rows = pl.ds(pl.multiple_of(t * W, W), W)
+        return (block * mixg_v[t]).astype(BF16), rows, square
+
+    def project(part_of, i):
+        gained, rows, _ = part_of
+        return jnp.dot(gained, proj_v[i, rows, :], preferred_element_type=F32)
+
+    def spread_out(i, total):
         for h in range(H):
             part[i, :, h, :] = total[:, h * DK : (h + 1) * DK]
         for k in range(K):
             part_send[i, k] = part[i, k * RL : (k + 1) * RL].reshape(RL * H, DK).astype(BF16)
-        for dk in hops[::-1]:
-            k, t = other(dk, 0)[0], tp
+
+    def scatter(i):
+        for j in hops[::-1]:
+            k = hop(j)
             sent.append(
                 send(
                     part_send.at[i, k],
                     part_recv.at[i, kv],
-                    part_ss.at[i, dk],
+                    part_ss.at[i, j],
                     part_rs.at[i, kv],
                     k,
-                    t,
+                    tp,
                 )
             )
+
+    mine = features(tp)
+    early = []
+    for i in range(2):
+        c_proj[i].wait()
+        early.append(project(mine, i))
+    swap.wait_recv()
+    theirs = features(1 - tp)
+    square = jnp.broadcast_to(mine[2] + theirs[2], (R, DK))
+    for k in range(K):
+        sq_send[k] = square[k * RL : (k + 1) * RL]
+    totals = [early[i] + project(theirs, i) for i in range(2)]
+    spread_out(0, totals[0])
+    spread_out(1, totals[1])
+
+    @pl.when(tp == 0)
+    def _():
+        pl.semaphore_wait(barrier, K * T - 1)
+        swap.start()
+
+    for j in hops[::-1]:
+        k = hop(j)
+        sent.append(send(sq_send.at[k], sq_recv.at[kv], sq_ss.at[j], sq_rs.at[kv], k, tp))
+    scatter(0)
+    scatter(1)
+    c_wout = load(10, w_out, wout_v)
+    c_wgate = load(11, w_gate, wgate_v)
+    c_wup = load(12, w_up, wup_v)
+    c_wdown = load(13, w_down, wdown_v)
+    totals = []
+    for i in range(2, 4):
+        c_proj[i].wait()
+        totals.append(project(mine, i) + project(theirs, i))
+    for i in range(2, 4):
+        spread_out(i, totals[i - 2])
+        scatter(i)
 
     c_floor.wait()
     c_hgain.wait()
@@ -355,6 +382,17 @@
         copy.wait_send()
 
 
+def flush(result_v, state_v, result, new_state, sem):
+    copies = [
+        pltpu.make_async_copy(state_v, new_state, sem.at[0]),
+        pltpu.make_async_copy(result_v, result, sem.at[1]),
+    ]
+    for copy in copies:
+        copy.start()
+    for copy in copies:
+        copy.wait()
+
+
 def body(
     tokens,
     past_state,
@@ -373,6 +411,7 @@
 ):
     K = lax.axis_size("kv")
     T = lax.axis_size("tp")
+    assert T == 2
     n = K * T
     R, W = tokens.shape
     RL, H, DK, DV = past_state.shape
@@ -395,7 +434,7 @@
     V = pltpu.VMEM
     dma = pltpu.SemaphoreType.DMA
     anywhere = pl.BlockSpec(memory_space=pl.ANY)
-    return pl.pallas_call(
+    outs = pl.pallas_call(
         functools.partial(kernel, K, T),
         out_shape=(
             pltpu.VMEM((R, W), BF16),
@@ -427,8 +466,8 @@
             V((n, R, W), BF16),
             V((n, R, W), BF16),
             dma((14,)),
-            dma((T,)),
-            dma((T,)),
+            dma,
+            dma,
             dma((K,)),
             dma((K,)),
             dma((4, K)),
@@ -444,6 +483,17 @@
             collective_id=0, has_side_effects=True, vmem_limit_bytes=60 * 1024 * 1024
         ),
     )(*args)
+    return pl.pallas_call(
+        flush,
+        out_shape=(
+            jax.ShapeDtypeStruct((R, W), BF16),
+            jax.ShapeDtypeStruct(past_state.shape, F32),
+        ),
+        in_specs=[pl.BlockSpec(memory_space=V)] * 2,
+        out_specs=(anywhere,) * 2,
+        scratch_shapes=[dma((2,))],
+        compiler_params=pltpu.CompilerParams(vmem_limit_bytes=1024 * 1024),
+    )(*outs)
 
 
 def solution(mesh):

time: 25.7 us -> 23.8 us (0.926)
  local copies, waits for them, and re-layouts: 1.56 us -> 0 us
  Pallas kernels: 23.3 us -> 23 us
    unnamed x2 -> x0, local copies, waits for them, and re-layouts: 1.56 us -> none
    pallas_call x1, Pallas kernels: 23.3 us -> 22 us  [body(): pl.pallas_call(functools.partial(kernel, K, T), out_shape=(pltpu.VMEM((R,...]
    pallas_call x0 -> x1, Pallas kernels: none -> 0.99 us  [body(): pl.pallas_call(flush, out_shape=(jax.ShapeDtypeStruct((R, W), BF16), jax....]
where the time goes in v2:
time: 23.8 us; the launch traced here: 23.6 us
  Pallas kernels  23 us (97%)
  between operations  0.64 us (3%)
    pallas_call x1, Pallas kernels, body(): pl.pallas_call(functools.partial(kernel, K, T), out_shape=(pltpu.VMEM((R,...  22 us
    pallas_call x1, Pallas kernels, body(): pl.pallas_call(flush, out_shape=(jax.ShapeDtypeStruct((R, W), BF16), jax....  0.99 us

profile of v2, /device:TPU:0, one launch (start us, length us, event | category | flops | bytes accessed | tf_op | source)
XLA Modules:
  0.0 23.6 jit_solution(14896124712691905269)
XLA Ops:
  0.6 22.0 %shard_map.149 = (bf16[8,256]{1,0:T(8,128)(2,1)S(1)}, f32[2,8,128,128]{3,2,1,0:T(8,128)S(1)}) custom-call(bf16[8,256]{1,0:T(8,128)(2,1)} %tokens.1, f32[2,8,128,128]{3,2,1,0:T(8,128)} %past.1, f32[2,1,256]{2,1,0:T(1,128)} %bitcast.10, bf16[512,1024]{1,0:T(8,128)(2,1)} %w_query.1, bf16[512,1024]{1,0:T(8,128)(2,1)} %w_forget.1, bf16[512,1024]{1,0:T(8,128)(2,1)} %w_value.1, ...), custom_call_target="tpu_custom_call" | custom-call | tf_op jit(solution)/shard_map/pallas_call | solution.py:437
  22.6 1.0 %shard_map.150 = (bf16[8,256]{1,0:T(8,128)(2,1)}, f32[2,8,128,128]{3,2,1,0:T(8,128)}) custom-call(bf16[8,256]{1,0:T(8,128)(2,1)S(1)} %get-tuple-element.4.result_v, f32[2,8,128,128]{3,2,1,0:T(8,128)S(1)} %get-tuple-element.5.state_v), custom_call_target="tpu_custom_call" | custom-call | tf_op jit(solution)/shard_map/pallas_call | solution.py:486

commit v3 on v2

--- a/solution.py
+++ b/solution.py
@@ -73,6 +73,8 @@
     sq_rs,
     part_ss,
     part_rs,
+    wout_ss,
+    wout_rs,
     mix_ss,
     mix_rs,
     mid_ss,
@@ -132,8 +134,8 @@
     signal(kv, 1 - tp)
     c_tok.wait()
 
-    def send(src, dst, ss, rs, k, t):
-        copy = pltpu.make_async_remote_copy(
+    def remote(src, dst, ss, rs, k, t):
+        return pltpu.make_async_remote_copy(
             src_ref=src,
             dst_ref=dst,
             send_sem=ss,
@@ -141,6 +143,9 @@
             device_id={"kv": k, "tp": t},
             device_id_type=MESH,
         )
+
+    def send(*args):
+        copy = remote(*args)
         copy.start()
         return copy
 
@@ -226,7 +231,7 @@
         sent.append(send(sq_send.at[k], sq_recv.at[kv], sq_ss.at[j], sq_rs.at[kv], k, tp))
     scatter(0)
     scatter(1)
-    c_wout = load(10, w_out, wout_v)
+    push = remote(w_out, wout_v.at[0], wout_ss, wout_rs, kv, 1)
     c_wgate = load(11, w_gate, wgate_v)
     c_wup = load(12, w_up, wup_v)
     c_wdown = load(13, w_down, wdown_v)
@@ -237,6 +242,14 @@
     for i in range(2, 4):
         spread_out(i, totals[i - 2])
         scatter(i)
+
+    @pl.when(tp == 0)
+    def _():
+        push.start()
+
+    @pl.when(tp == 1)
+    def _():
+        pltpu.make_async_copy(w_out, wout_v.at[1], local_sem.at[10]).start()
 
     c_floor.wait()
     c_hgain.wait()
@@ -287,10 +300,14 @@
     )
     mixed = normed * hgain_v[...] * silu(summed(3))
     mix_all[tp, kv] = mixed.astype(BF16)
-    for dk, dt in near[::-1]:
-        k, t = other(dk, dt)
-        slot = mix_all.at[tp, kv]
-        sent.append(send(slot, slot, mix_ss.at[dk, dt], mix_rs.at[kv, tp], k, t))
+    slot = mix_all.at[tp, kv]
+    for j in hops[::-1]:
+        sent.append(send(slot, slot, mix_ss.at[j], mix_rs.at[kv, tp], hop(j), 1))
+    aside = remote(slot, slot, mix_ss.at[0], mix_rs.at[kv, tp], kv, 1)
+
+    @pl.when(tp == 0)
+    def _():
+        aside.start()
 
     columns = forget.T
     for s in range(RL):
@@ -302,39 +319,57 @@
     def spread(t, k):
         mix_f[t, pl.ds(k * RL, RL)] = mix_all[t, k].astype(F32).reshape(RL, H, DV)
 
-    spread(tp, kv)
-    for dk, dt in near:
-        k, t = source(dk, dt)
-        arrived(mix_all.at[t, k], mix_ss.at[dk, dt], mix_rs.at[k, t])
-        spread(t, k)
-    every_head = jnp.concatenate(
-        [mix_f[t, :, h, :].astype(BF16) for t in range(T) for h in range(H)], axis=1
-    )
-    c_wout.wait()
-    middle = tok_v[tp].astype(F32) + jnp.dot(
-        every_head, wout_v[...], preferred_element_type=F32
-    )
-    middle = middle.astype(BF16)
-    mid_all[me] = middle
-    for dk, dt in near[::-1]:
-        k, t = other(dk, dt)
-        slot = mid_all.at[me]
-        sent.append(send(slot, slot, mid_ss.at[dk, dt], mid_rs.at[kv, tp], k, t))
+    given = []
+    for t in range(T):
+        slot = mid_all.at[kv * T + t]
+        for j in hops[::-1] + [0]:
+            for peer in range(1 if j == 0 else T):
+                given.append(
+                    remote(slot, slot, mid_ss.at[j, peer, t], mid_rs.at[kv, t], hop(j), peer)
+                )
+
+    @pl.when(tp == 1)
+    def _():
+        spread(1, kv)
+        arrived(mix_all.at[0, kv], mix_ss.at[0], mix_rs.at[kv, 0])
+        spread(0, kv)
+        for j in hops:
+            k = hop(j)
+            for t in range(T)[::-1]:
+                arrived(mix_all.at[t, k], mix_ss.at[j], mix_rs.at[k, t])
+                spread(t, k)
+        every_head = jnp.concatenate(
+            [mix_f[t, :, h, :].astype(BF16) for t in range(T) for h in range(H)], axis=1
+        )
+        pltpu.make_async_copy(w_out, wout_v.at[1], local_sem.at[10]).wait()
+        arrived(wout_v.at[0], wout_ss, wout_rs)
+        for t in range(T):
+            middle = tok_v[t].astype(F32) + jnp.dot(
+                every_head, wout_v[t], preferred_element_type=F32
+            )
+            mid_all[kv * T + t] = middle.astype(BF16)
+            for copy in given[t * len(given) // T : (t + 1) * len(given) // T]:
+                copy.start()
 
     c_mlpg.wait()
     square = jnp.zeros((R, 1), F32)
     gate = None
     if W % 128 == 0:
-        groups = [[peer] for peer in [(0, 0)] + near]
+        groups = [[(j, t)] for j in [0] + hops for t in range(T)]
     else:
-        groups = [[(dk, dt) for dt in range(T)] for dk in [0] + hops]
+        groups = [[(j, t) for t in range(T)] for j in [0] + hops]
     for group in groups:
-        for dk, dt in group:
-            k, t = source(dk, dt)
-            if dk or dt:
-                arrived(mid_all.at[k * T + t], mid_ss.at[dk, dt], mid_rs.at[k, t])
-        k, t = source(*group[0])
-        j = k * T + (t if len(group) == 1 else 0)
+        k = hop(group[0][0])
+        for j, t in group:
+            if j:
+                arrived(mid_all.at[k * T + t], mid_ss.at[j, 0, t], mid_rs.at[k, t])
+            else:
+
+                @pl.when(tp == 0)
+                def _(t=t):
+                    arrived(mid_all.at[kv * T + t], mid_ss.at[0, 0, t], mid_rs.at[kv, t])
+
+        j = k * T + group[0][1]
         blocks = []
         for i in range(len(group)):
             block = mid_all[j + i].astype(F32)
@@ -377,9 +412,19 @@
         j = k * T + t
         arrived(term_recv.at[j], term_ss.at[dk, dt], term_rs.at[k, t])
         total = total + term_recv[j].astype(F32)
-    result[...] = (middle.astype(F32) + total).astype(BF16)
+    result[...] = (mid_all[me].astype(F32) + total).astype(BF16)
     for copy in sent:
         copy.wait_send()
+
+    @pl.when(tp == 0)
+    def _():
+        push.wait_send()
+        aside.wait_send()
+
+    @pl.when(tp == 1)
+    def _():
+        for copy in given:
+            copy.wait_send()
 
 
 def flush(result_v, state_v, result, new_state, sem):
@@ -449,7 +494,7 @@
             V((4,) + w_query.shape, BF16),
             V((H, DK), F32),
             V((1, DV), F32),
-            V(w_out.shape, BF16),
+            V((T,) + w_out.shape, BF16),
             V((n, 1, W), F32),
             V(w_gate.shape[::-1], BF16),
             V(w_up.shape[::-1], BF16),
@@ -472,9 +517,11 @@
             dma((K,)),
             dma((4, K)),
             dma((4, K)),
+            dma,
+            dma,
+            dma((K,)),
             dma((K, T)),
-            dma((K, T)),
-            dma((K, T)),
+            dma((K, T, T)),
             dma((K, T)),
             dma((K, T)),
             dma((K, T)),

time: 23.8 us -> 23.1 us (0.971)
  Pallas kernels: 23 us -> 22.3 us
    pallas_call x1, Pallas kernels: 22 us -> 21.3 us  [body(): pl.pallas_call(functools.partial(kernel, K, T), out_shape=(pltpu.VMEM((R,...]
where the time goes in v3:
time: 23.1 us; the launch traced here: 22.9 us
  Pallas kernels  22.3 us (97%)
  between operations  0.64 us (3%)
    pallas_call x1, Pallas kernels, body(): pl.pallas_call(functools.partial(kernel, K, T), out_shape=(pltpu.VMEM((R,...  21.3 us
    pallas_call x1, Pallas kernels, body(): pl.pallas_call(flush, out_shape=(jax.ShapeDtypeStruct((R, W), BF16), jax....  0.99 us

profile of v3, /device:TPU:0, one launch (start us, length us, event | category | flops | bytes accessed | tf_op | source)
XLA Modules:
  0.0 22.9 jit_solution(11477390992785024988)
XLA Ops:
  0.6 21.3 %shard_map.149 = (bf16[8,256]{1,0:T(8,128)(2,1)S(1)}, f32[2,8,128,128]{3,2,1,0:T(8,128)S(1)}) custom-call(bf16[8,256]{1,0:T(8,128)(2,1)} %tokens.1, f32[2,8,128,128]{3,2,1,0:T(8,128)} %past.1, f32[2,1,256]{2,1,0:T(1,128)} %bitcast.10, bf16[512,1024]{1,0:T(8,128)(2,1)} %w_query.1, bf16[512,1024]{1,0:T(8,128)(2,1)} %w_forget.1, bf16[512,1024]{1,0:T(8,128)(2,1)} %w_value.1, ...), custom_call_target="tpu_custom_call" | custom-call | tf_op jit(solution)/shard_map/pallas_call | solution.py:482
  22.0 1.0 %shard_map.150 = (bf16[8,256]{1,0:T(8,128)(2,1)}, f32[2,8,128,128]{3,2,1,0:T(8,128)}) custom-call(bf16[8,256]{1,0:T(8,128)(2,1)S(1)} %get-tuple-element.4.result_v, f32[2,8,128,128]{3,2,1,0:T(8,128)S(1)} %get-tuple-element.5.state_v), custom_call_target="tpu_custom_call" | custom-call | tf_op jit(solution)/shard_map/pallas_call | solution.py:533

commit v4 on v3

--- a/solution.py
+++ b/solution.py
@@ -60,19 +60,25 @@
     part,
     part_send,
     part_recv,
-    split_v,
+    round_v,
     mix_all,
     mix_f,
     mid_all,
     term_send,
     term_recv,
     local_sem,
+    ready,
     tok_ss,
     tok_rs,
     sq_ss,
     sq_rs,
     part_ss,
     part_rs,
+    again_ss,
+    floor_ss,
+    floor_rs,
+    past_ss,
+    past_rs,
     wout_ss,
     wout_rs,
     mix_ss,
@@ -120,7 +126,7 @@
         for i, w in enumerate((w_forget, w_query, w_value, w_gate_out))
     ]
     c_past = load(6, past, past_v)
-    c_floor = load(7, floor_logits, floor_v)
+    c_floor = load(7, floor_logits, floor_v.at[tp])
     c_hgain = load(8, head_gain, hgain_v)
     c_mlpg = load(9, mlp_gain, mlpg_v)
 
@@ -131,7 +137,11 @@
 
     for j in hops[::-1]:
         signal(hop(j), 0)
-    signal(kv, 1 - tp)
+
+    @pl.when(tp == 0)
+    def _():
+        signal(kv, 1)
+
     c_tok.wait()
 
     def remote(src, dst, ss, rs, k, t):
@@ -173,6 +183,12 @@
     @pl.when(tp == 1)
     def _():
         pl.semaphore_wait(barrier, 1)
+        pl.semaphore_signal(ready, inc=1, device_id={"kv": kv, "tp": 0}, device_id_type=MESH)
+        swap.start()
+
+    @pl.when(tp == 0)
+    def _():
+        pl.semaphore_wait(ready, 1)
         swap.start()
 
     c_mixg.wait()
@@ -199,32 +215,49 @@
             sent.append(
                 send(
                     part_send.at[i, k],
-                    part_recv.at[i, kv],
+                    part_recv.at[tp, i, kv],
                     part_ss.at[i, j],
-                    part_rs.at[i, kv],
+                    part_rs.at[tp, i, kv],
                     k,
-                    tp,
+                    1,
                 )
             )
-
+        own = remote(
+            part_send.at[i, kv],
+            part_recv.at[0, i, kv],
+            part_ss.at[i, 0],
+            part_rs.at[0, i, kv],
+            kv,
+            1,
+        )
+        from_zero.append(own)
+
+        @pl.when(tp == 0)
+        def _():
+            own.start()
+
+    from_zero = []
     mine = features(tp)
-    early = []
-    for i in range(2):
-        c_proj[i].wait()
-        early.append(project(mine, i))
     swap.wait_recv()
     theirs = features(1 - tp)
     square = jnp.broadcast_to(mine[2] + theirs[2], (R, DK))
     for k in range(K):
         sq_send[k] = square[k * RL : (k + 1) * RL]
-    totals = [early[i] + project(theirs, i) for i in range(2)]
+    totals = []
+    for i in range(2):
+        c_proj[i].wait()
+        totals.append(project(mine, i) + project(theirs, i))
     spread_out(0, totals[0])
     spread_out(1, totals[1])
 
     @pl.when(tp == 0)
     def _():
-        pl.semaphore_wait(barrier, K * T - 1)
-        swap.start()
+        pl.semaphore_wait(barrier, (K - 1) * T)
+        pl.semaphore_signal(ready, inc=1, device_id={"kv": kv, "tp": 1}, device_id_type=MESH)
+
+    @pl.when(tp == 1)
+    def _():
+        pl.semaphore_wait(ready, 1)
 
     for j in hops[::-1]:
         k = hop(j)
@@ -243,26 +276,41 @@
         spread_out(i, totals[i - 2])
         scatter(i)
 
-    @pl.when(tp == 0)
-    def _():
-        push.start()
-
-    @pl.when(tp == 1)
-    def _():
-        pltpu.make_async_copy(w_out, wout_v.at[1], local_sem.at[10]).start()
-
-    c_floor.wait()
-    c_hgain.wait()
-    lower = sigmoid(floor_v[...])
-    lower = jnp.concatenate([lower] * RL, axis=0)
+    for i in (0, 2):
+        for j in hops[::-1]:
+            k = hop(j)
+            from_zero.append(
+                remote(
+                    part_send.at[i, k],
+                    part_recv.at[0, i, kv],
+                    again_ss.at[i // 2, j],
+                    part_rs.at[0, i, kv],
+                    k,
+                    0,
+                )
+            )
     c_past.wait()
     for s in range(RL):
         for h in range(H):
             rows = pl.ds((s * H + h) * DK, DK)
-            block = past_v[s, h]
-            high = block.astype(BF16)
-            split_v[rows, :DV] = high
-            split_v[rows, DV:] = (block - high.astype(F32)).astype(BF16)
+            round_v[tp, rows, :] = past_v[s, h].astype(BF16)
+    pushes = [
+        remote(floor_logits, floor_v.at[0], floor_ss, floor_rs, kv, 1),
+        remote(round_v.at[0], round_v.at[0], past_ss, past_rs, kv, 1),
+        push,
+    ]
+
+    @pl.when(tp == 0)
+    def _():
+        for copy in pushes[:2] + from_zero[4:] + pushes[2:]:
+            copy.start()
+
+    @pl.when(tp == 1)
+    def _():
+        pltpu.make_async_copy(w_out, wout_v.at[1], local_sem.at[10]).start()
+
+    c_floor.wait()
+    c_hgain.wait()
     square = sq_send[kv]
     for dk in hops:
         k, t = source(dk, 0)
@@ -273,42 +321,79 @@
         [jnp.broadcast_to(row_scale[s : s + 1], (H, DK)) for s in range(RL)], axis=0
     )
 
-    def summed(i):
-        total = part[i, pl.ds(kv * RL, RL)].reshape(RL * H, DK)
-        for dk in hops:
-            k, t = source(dk, 0)
-            arrived(part_recv.at[i, k], part_ss.at[i, dk], part_rs.at[i, k])
-            total = total + part_recv[i, k].astype(F32)
+    def own_part(i):
+        return part[i, pl.ds(kv * RL, RL)].reshape(RL * H, DK)
+
+    def from_peers(u, i):
+        for j in hops:
+            k = hop(j)
+            arrived(part_recv.at[u, i, k], part_ss.at[i, j], part_rs.at[u, i, k])
+
+    def summed(u, i, total):
+        for j in hops:
+            total = total + part_recv[u, i, hop(j)].astype(F32)
         return total * row_scale
 
-    forget = lower + (1.0 - lower) * sigmoid(summed(0))
-    activ = silu(summed(1))
-    weight = activ * forget
-    high = weight.astype(BF16).astype(F32)
-    weight = jnp.concatenate([high, weight - high], axis=0)
-    owner = lax.rem(lax.broadcasted_iota(jnp.int32, weight.shape, 0), RL * H)
-    left = jnp.concatenate(
-        [jnp.where(owner == i, weight, 0.0).astype(BF16) for i in range(RL * H)], axis=1
-    )
-    wide = jnp.dot(left, split_v[...], preferred_element_type=F32)
-    head_out = wide[: RL * H, :DV] + (wide[: RL * H, DV:] + wide[RL * H :, :DV])
-    rest = jnp.sum(activ * (1.0 - forget), axis=1, keepdims=True)
-    value = summed(2)
-    head_out = head_out + value * rest
-    normed = head_out * lax.rsqrt(
-        jnp.mean(head_out * head_out, axis=1, keepdims=True) + epsilon
-    )
-    mixed = normed * hgain_v[...] * silu(summed(3))
-    mix_all[tp, kv] = mixed.astype(BF16)
-    slot = mix_all.at[tp, kv]
-    for j in hops[::-1]:
-        sent.append(send(slot, slot, mix_ss.at[j], mix_rs.at[kv, tp], hop(j), 1))
-    aside = remote(slot, slot, mix_ss.at[0], mix_rs.at[kv, tp], kv, 1)
+    def from_zeros(i):
+        arrived(part_recv.at[0, i, kv], part_ss.at[i, 0], part_rs.at[0, i, kv])
+        from_peers(0, i)
+
+    def total_of(u, i):
+        own = part_recv[0, i, kv].astype(F32) if u == 0 else own_part(i)
+        return summed(u, i, own)
+
+    def forget_of(u, total):
+        lower = sigmoid(floor_v[u])
+        lower = jnp.concatenate([lower] * RL, axis=0)
+        return lower + (1.0 - lower) * sigmoid(total)
+
+    owner = lax.broadcasted_iota(jnp.int32, (RL * H, DK), 0)
+
+    def weighted(u, forget, activ):
+        weight = activ * forget
+        left = jnp.concatenate(
+            [jnp.where(owner == i, weight, 0.0).astype(BF16) for i in range(RL * H)], axis=1
+        )
+        return (
+            jnp.dot(left, round_v[u], preferred_element_type=F32),
+            jnp.sum(activ * (1.0 - forget), axis=1, keepdims=True),
+        )
+
+    def gated(u, head_out, gate_pre):
+        normed = head_out * lax.rsqrt(
+            jnp.mean(head_out * head_out, axis=1, keepdims=True) + epsilon
+        )
+        mix_all[kv, u] = (normed * hgain_v[...] * silu(gate_pre)).astype(BF16)
+
+    from_peers(tp, 0)
+    forget = forget_of(tp, summed(tp, 0, own_part(0)))
+    mix_sends = [
+        remote(mix_all.at[kv], mix_all.at[kv], mix_ss.at[j], mix_rs.at[kv], hop(j), 1)
+        for j in hops[::-1]
+    ]
 
     @pl.when(tp == 0)
     def _():
-        aside.start()
-
+        from_peers(0, 2)
+
+    @pl.when(tp == 1)
+    def _():
+        arrived(floor_v.at[0], floor_ss, floor_rs)
+        arrived(round_v.at[0], past_ss, past_rs)
+        from_zeros(0)
+        from_zeros(1)
+        from_peers(1, 1)
+        zero, zero_rest = weighted(0, forget_of(0, total_of(0, 0)), silu(total_of(0, 1)))
+        one, one_rest = weighted(1, forget, silu(total_of(1, 1)))
+        for i in (2, 3):
+            from_zeros(i)
+            from_peers(1, i)
+        gated(0, zero + total_of(0, 2) * zero_rest, total_of(0, 3))
+        gated(1, one + total_of(1, 2) * one_rest, total_of(1, 3))
+        for copy in mix_sends:
+            copy.start()
+
+    value = summed(tp, 2, own_part(2))
     columns = forget.T
     for s in range(RL):
         for h in range(H):
@@ -317,7 +402,7 @@
             new_state[s, h] = row + columns[:, i : i + 1] * (past_v[s, h] - row)
 
     def spread(t, k):
-        mix_f[t, pl.ds(k * RL, RL)] = mix_all[t, k].astype(F32).reshape(RL, H, DV)
+        mix_f[t, pl.ds(k * RL, RL)] = mix_all[k, t].astype(F32).reshape(RL, H, DV)
 
     given = []
     for t in range(T):
@@ -330,13 +415,11 @@
 
     @pl.when(tp == 1)
     def _():
-        spread(1, kv)
-        arrived(mix_all.at[0, kv], mix_ss.at[0], mix_rs.at[kv, 0])
-        spread(0, kv)
-        for j in hops:
+        for j in [0] + hops:
             k = hop(j)
-            for t in range(T)[::-1]:
-                arrived(mix_all.at[t, k], mix_ss.at[j], mix_rs.at[k, t])
+            if j:
+                arrived(mix_all.at[k], mix_ss.at[j], mix_rs.at[k])
+            for t in range(T):
                 spread(t, k)
         every_head = jnp.concatenate(
             [mix_f[t, :, h, :].astype(BF16) for t in range(T) for h in range(H)], axis=1
@@ -418,12 +501,12 @@
 
     @pl.when(tp == 0)
     def _():
-        push.wait_send()
-        aside.wait_send()
+        for copy in from_zero + pushes:
+            copy.wait_send()
 
     @pl.when(tp == 1)
     def _():
-        for copy in given:
+        for copy in mix_sends + given:
             copy.wait_send()
 
 
@@ -492,7 +575,7 @@
             V(past_state.shape, F32),
             V((T, 1, W), F32),
             V((4,) + w_query.shape, BF16),
-            V((H, DK), F32),
+            V((T, H, DK), F32),
             V((1, DV), F32),
             V((T,) + w_out.shape, BF16),
             V((n, 1, W), F32),
@@ -503,24 +586,30 @@
             V((K, RL, DK), F32),
             V((4, R, H, DK), F32),
             V((4, K, RL * H, DK), BF16),
-            V((4, K, RL * H, DK), BF16),
-            V((RL * H * DK, 2 * DV), BF16),
-            V((T, K, RL * H, DV), BF16),
+            V((T, 4, K, RL * H, DK), BF16),
+            V((T, RL * H * DK, DV), BF16),
+            V((K, T, RL * H, DV), BF16),
             V((T, R, H, DV), F32),
             V((n, R, W), BF16),
             V((n, R, W), BF16),
             V((n, R, W), BF16),
             dma((14,)),
+            pltpu.SemaphoreType.REGULAR,
             dma,
             dma,
             dma((K,)),
             dma((K,)),
             dma((4, K)),
-            dma((4, K)),
+            dma((T, 4, K)),
+            dma((2, K)),
+            dma,
+            dma,
+            dma,
+            dma,
             dma,
             dma,
             dma((K,)),
-            dma((K, T)),
+            dma((K,)),
             dma((K, T, T)),
             dma((K, T)),
             dma((K, T)),

time: 23.1 us -> 22.8 us (0.987)
  Pallas kernels: 22.3 us -> 22 us
    pallas_call x1, Pallas kernels: 21.3 us -> 21 us  [body(): pl.pallas_call(functools.partial(kernel, K, T), out_shape=(pltpu.VMEM((R,...]
where the time goes in v4:
time: 22.8 us; the launch traced here: 22.6 us
  Pallas kernels  22 us (96%)
  between operations  0.64 us (3%)
    pallas_call x1, Pallas kernels, body(): pl.pallas_call(functools.partial(kernel, K, T), out_shape=(pltpu.VMEM((R,...  21 us
    pallas_call x1, Pallas kernels, body(): pl.pallas_call(flush, out_shape=(jax.ShapeDtypeStruct((R, W), BF16), jax....  0.99 us

profile of v4, /device:TPU:0, one launch (start us, length us, event | category | flops | bytes accessed | tf_op | source)
XLA Modules:
  0.0 22.6 jit_solution(930230076885464200)
XLA Ops:
  0.6 21.0 %shard_map.149 = (bf16[8,256]{1,0:T(8,128)(2,1)S(1)}, f32[2,8,128,128]{3,2,1,0:T(8,128)S(1)}) custom-call(bf16[8,256]{1,0:T(8,128)(2,1)} %tokens.1, f32[2,8,128,128]{3,2,1,0:T(8,128)} %past.1, f32[2,1,256]{2,1,0:T(1,128)} %bitcast.10, bf16[512,1024]{1,0:T(8,128)(2,1)} %w_query.1, bf16[512,1024]{1,0:T(8,128)(2,1)} %w_forget.1, bf16[512,1024]{1,0:T(8,128)(2,1)} %w_value.1, ...), custom_call_target="tpu_custom_call" | custom-call | tf_op jit(solution)/shard_map/pallas_call | solution.py:565
  21.6 1.0 %shard_map.150 = (bf16[8,256]{1,0:T(8,128)(2,1)}, f32[2,8,128,128]{3,2,1,0:T(8,128)}) custom-call(bf16[8,256]{1,0:T(8,128)(2,1)S(1)} %get-tuple-element.4.result_v, f32[2,8,128,128]{3,2,1,0:T(8,128)S(1)} %get-tuple-element.5.state_v), custom_call_target="tpu_custom_call" | custom-call | tf_op jit(solution)/shard_map/pallas_call | solution.py:622

commit v5 on v4

--- a/solution.py
+++ b/solution.py
@@ -19,10 +19,6 @@
 
 def silu(a):
     return a / (1.0 + jnp.exp(-a))
-
-
-def dot_t(a, b):
-    return lax.dot_general(a, b, (((1,), (1,)), ((), ())), preferred_element_type=F32)
 
 
 def kernel(
@@ -54,6 +50,8 @@
     mlpg_v,
     wgate_v,
     wup_v,
+    gatet_v,
+    upt_v,
     wdown_v,
     sq_send,
     sq_recv,
@@ -142,6 +140,11 @@
     def _():
         signal(kv, 1)
 
+    @pl.when(tp == 1)
+    def _():
+        pl.semaphore_wait(barrier, 1)
+        pl.semaphore_signal(ready, inc=1, device_id={"kv": kv, "tp": 0}, device_id_type=MESH)
+
     c_tok.wait()
 
     def remote(src, dst, ss, rs, k, t):
@@ -169,7 +172,17 @@
             device_id_type=MESH,
         ).wait_recv()
 
-    sent = []
+    def left(src, ss):
+        pltpu.make_async_remote_copy(
+            src_ref=src,
+            dst_ref=src,
+            send_sem=ss,
+            recv_sem=tok_rs,
+            device_id={"kv": kv, "tp": 1 - tp},
+            device_id_type=MESH,
+        ).wait_send()
+
+    most = pl.ds(0, K - 1)
     swap = pltpu.make_async_remote_copy(
         src_ref=tok_v.at[tp],
         dst_ref=tok_v.at[tp],
@@ -178,19 +191,12 @@
         device_id={"kv": kv, "tp": 1 - tp},
         device_id_type=MESH,
     )
-    sent.append(swap)
-
-    @pl.when(tp == 1)
-    def _():
-        pl.semaphore_wait(barrier, 1)
-        pl.semaphore_signal(ready, inc=1, device_id={"kv": kv, "tp": 0}, device_id_type=MESH)
-        swap.start()
 
     @pl.when(tp == 0)
     def _():
         pl.semaphore_wait(ready, 1)
-        swap.start()
-
+
+    swap.start()
     c_mixg.wait()
 
     def features(t):
@@ -212,41 +218,39 @@
     def scatter(i):
         for j in hops[::-1]:
             k = hop(j)
-            sent.append(
-                send(
-                    part_send.at[i, k],
-                    part_recv.at[tp, i, kv],
-                    part_ss.at[i, j],
-                    part_rs.at[tp, i, kv],
-                    k,
-                    1,
-                )
+            send(
+                part_send.at[i, k],
+                part_recv.at[tp, i, kv],
+                part_ss,
+                part_rs.at[tp, i // 2],
+                k,
+                1,
             )
         own = remote(
             part_send.at[i, kv],
             part_recv.at[0, i, kv],
-            part_ss.at[i, 0],
-            part_rs.at[0, i, kv],
+            part_ss,
+            part_rs.at[0, i // 2],
             kv,
             1,
         )
-        from_zero.append(own)
 
         @pl.when(tp == 0)
         def _():
             own.start()
 
-    from_zero = []
+    again = []
     mine = features(tp)
+    early = []
+    for i in range(2):
+        c_proj[i].wait()
+        early.append(project(mine, i))
     swap.wait_recv()
     theirs = features(1 - tp)
     square = jnp.broadcast_to(mine[2] + theirs[2], (R, DK))
     for k in range(K):
         sq_send[k] = square[k * RL : (k + 1) * RL]
-    totals = []
-    for i in range(2):
-        c_proj[i].wait()
-        totals.append(project(mine, i) + project(theirs, i))
+    totals = [early[i] + project(theirs, i) for i in range(2)]
     spread_out(0, totals[0])
     spread_out(1, totals[1])
 
@@ -261,7 +265,7 @@
 
     for j in hops[::-1]:
         k = hop(j)
-        sent.append(send(sq_send.at[k], sq_recv.at[kv], sq_ss.at[j], sq_rs.at[kv], k, tp))
+        send(sq_send.at[k], sq_recv.at[kv], sq_ss, sq_rs, k, tp)
     scatter(0)
     scatter(1)
     push = remote(w_out, wout_v.at[0], wout_ss, wout_rs, kv, 1)
@@ -279,12 +283,12 @@
     for i in (0, 2):
         for j in hops[::-1]:
             k = hop(j)
-            from_zero.append(
+            again.append(
                 remote(
                     part_send.at[i, k],
                     part_recv.at[0, i, kv],
-                    again_ss.at[i // 2, j],
-                    part_rs.at[0, i, kv],
+                    again_ss,
+                    part_rs.at[0, i // 2],
                     k,
                     0,
                 )
@@ -302,7 +306,7 @@
 
     @pl.when(tp == 0)
     def _():
-        for copy in pushes[:2] + from_zero[4:] + pushes[2:]:
+        for copy in pushes[:2] + again + pushes[2:]:
             copy.start()
 
     @pl.when(tp == 1)
@@ -312,10 +316,9 @@
     c_floor.wait()
     c_hgain.wait()
     square = sq_send[kv]
-    for dk in hops:
-        k, t = source(dk, 0)
-        arrived(sq_recv.at[k], sq_ss.at[dk], sq_rs.at[k])
-        square = square + sq_recv[k]
+    arrived(sq_recv.at[most], sq_ss, sq_rs)
+    for j in hops:
+        square = square + sq_recv[hop(j)]
     row_scale = lax.rsqrt(square / D + epsilon)
     row_scale = jnp.concatenate(
         [jnp.broadcast_to(row_scale[s : s + 1], (H, DK)) for s in range(RL)], axis=0
@@ -324,19 +327,15 @@
     def own_part(i):
         return part[i, pl.ds(kv * RL, RL)].reshape(RL * H, DK)
 
-    def from_peers(u, i):
-        for j in hops:
-            k = hop(j)
-            arrived(part_recv.at[u, i, k], part_ss.at[i, j], part_rs.at[u, i, k])
+    def both(half):
+        pair = pl.ds(2 * half, 2)
+        arrived(part_recv.at[0, pair], part_ss, part_rs.at[0, half])
+        arrived(part_recv.at[1, pair, most], part_ss, part_rs.at[1, half])
 
     def summed(u, i, total):
         for j in hops:
             total = total + part_recv[u, i, hop(j)].astype(F32)
         return total * row_scale
-
-    def from_zeros(i):
-        arrived(part_recv.at[0, i, kv], part_ss.at[i, 0], part_rs.at[0, i, kv])
-        from_peers(0, i)
 
     def total_of(u, i):
         own = part_recv[0, i, kv].astype(F32) if u == 0 else own_part(i)
@@ -365,41 +364,41 @@
         )
         mix_all[kv, u] = (normed * hgain_v[...] * silu(gate_pre)).astype(BF16)
 
-    from_peers(tp, 0)
+    @pl.when(tp == 0)
+    def _():
+        arrived(part_recv.at[0, 0, most], part_ss, part_rs.at[0, 0])
+        arrived(part_recv.at[0, 2, most], part_ss, part_rs.at[0, 1])
+
+    @pl.when(tp == 1)
+    def _():
+        both(0)
+
     forget = forget_of(tp, summed(tp, 0, own_part(0)))
     mix_sends = [
-        remote(mix_all.at[kv], mix_all.at[kv], mix_ss.at[j], mix_rs.at[kv], hop(j), 1)
+        remote(mix_all.at[kv], mix_all.at[kv], mix_ss, mix_rs.at[kv], hop(j), 1)
         for j in hops[::-1]
     ]
 
-    @pl.when(tp == 0)
-    def _():
-        from_peers(0, 2)
-
     @pl.when(tp == 1)
     def _():
         arrived(floor_v.at[0], floor_ss, floor_rs)
         arrived(round_v.at[0], past_ss, past_rs)
-        from_zeros(0)
-        from_zeros(1)
-        from_peers(1, 1)
         zero, zero_rest = weighted(0, forget_of(0, total_of(0, 0)), silu(total_of(0, 1)))
         one, one_rest = weighted(1, forget, silu(total_of(1, 1)))
-        for i in (2, 3):
-            from_zeros(i)
-            from_peers(1, i)
+        both(1)
         gated(0, zero + total_of(0, 2) * zero_rest, total_of(0, 3))
         gated(1, one + total_of(1, 2) * one_rest, total_of(1, 3))
         for copy in mix_sends:
             copy.start()
 
-    value = summed(tp, 2, own_part(2))
-    columns = forget.T
-    for s in range(RL):
-        for h in range(H):
-            i = s * H + h
-            row = value[i : i + 1, :]
-            new_state[s, h] = row + columns[:, i : i + 1] * (past_v[s, h] - row)
+    def turn(copy, src, dst):
+        copy.wait()
+        step = 256 if D % 256 == 0 else D
+        for c in range(0, D, step):
+            dst[c : c + step, :] = src[:, c : c + step].T
+
+    turn(c_wgate, wgate_v, gatet_v)
+    turn(c_wup, wup_v, upt_v)
 
     def spread(t, k):
         mix_f[t, pl.ds(k * RL, RL)] = mix_all[k, t].astype(F32).reshape(RL, H, DV)
@@ -410,7 +409,7 @@
         for j in hops[::-1] + [0]:
             for peer in range(1 if j == 0 else T):
                 given.append(
-                    remote(slot, slot, mid_ss.at[j, peer, t], mid_rs.at[kv, t], hop(j), peer)
+                    remote(slot, slot, mid_ss.at[t], mid_rs.at[kv, t], hop(j), peer)
                 )
 
     @pl.when(tp == 1)
@@ -418,7 +417,7 @@
         for j in [0] + hops:
             k = hop(j)
             if j:
-                arrived(mix_all.at[k], mix_ss.at[j], mix_rs.at[k])
+                arrived(mix_all.at[k], mix_ss, mix_rs.at[k])
             for t in range(T):
                 spread(t, k)
         every_head = jnp.concatenate(
@@ -445,12 +444,12 @@
         k = hop(group[0][0])
         for j, t in group:
             if j:
-                arrived(mid_all.at[k * T + t], mid_ss.at[j, 0, t], mid_rs.at[k, t])
+                arrived(mid_all.at[k * T + t], mid_ss.at[t], mid_rs.at[k, t])
             else:
 
                 @pl.when(tp == 0)
                 def _(t=t):
-                    arrived(mid_all.at[kv * T + t], mid_ss.at[0, 0, t], mid_rs.at[kv, t])
+                    arrived(mid_all.at[kv * T + t], mid_ss.at[t], mid_rs.at[kv, t])
 
         j = k * T + group[0][1]
         blocks = []
@@ -461,12 +460,8 @@
         block = jnp.concatenate(blocks, axis=1) if len(blocks) > 1 else blocks[0]
         width = len(group) * W
         lanes = pl.ds(pl.multiple_of(j * W, width), width)
-        if gate is None:
-            c_wgate.wait()
-        g = dot_t(block, wgate_v[:, lanes])
-        if gate is None:
-            c_wup.wait()
-        u = dot_t(block, wup_v[:, lanes])
+        g = jnp.dot(block, gatet_v[lanes, :], preferred_element_type=F32)
+        u = jnp.dot(block, upt_v[lanes, :], preferred_element_type=F32)
         gate, upward = (g, u) if gate is None else (gate + g, upward + u)
     mlp_scale = lax.rsqrt(square / D + epsilon)
     hidden = (silu(gate * mlp_scale) * (upward * mlp_scale)).astype(BF16)
@@ -479,35 +474,38 @@
             term_send[k * T + t] = chunk[:, t * W : (t + 1) * W]
         for dt in range(0 if dk else 1, T):
             _, t = other(dk, dt)
-            sent.append(
-                send(
-                    term_send.at[k * T + t],
-                    term_recv.at[me],
-                    term_ss.at[dk, dt],
-                    term_rs.at[kv, tp],
-                    k,
-                    t,
-                )
-            )
+            send(term_send.at[k * T + t], term_recv.at[me], term_ss, term_rs, k, t)
+    value = summed(tp, 2, own_part(2))
+    columns = forget.T
+    for s in range(RL):
+        for h in range(H):
+            i = s * H + h
+            row = value[i : i + 1, :]
+            new_state[s, h] = row + columns[:, i : i + 1] * (past_v[s, h] - row)
+
     total = term_send[me].astype(F32)
+    arrived(term_recv.at[pl.ds(0, K * T - 1)], term_ss, term_rs)
     for dk, dt in near:
         k, t = source(dk, dt)
-        j = k * T + t
-        arrived(term_recv.at[j], term_ss.at[dk, dt], term_rs.at[k, t])
-        total = total + term_recv[j].astype(F32)
+        total = total + term_recv[k * T + t].astype(F32)
     result[...] = (mid_all[me].astype(F32) + total).astype(BF16)
-    for copy in sent:
-        copy.wait_send()
+    swap.wait_send()
+    left(sq_send.at[most], sq_ss)
+    left(term_send.at[pl.ds(0, K * T - 1)], term_ss)
 
     @pl.when(tp == 0)
     def _():
-        for copy in from_zero + pushes:
+        left(part_send, part_ss)
+        left(part_send.at[pl.ds(0, 2), most], again_ss)
+        for copy in pushes:
             copy.wait_send()
 
     @pl.when(tp == 1)
     def _():
-        for copy in mix_sends + given:
-            copy.wait_send()
+        left(part_send.at[:, most], part_ss)
+        left(mix_all.at[most], mix_ss)
+        for t in range(T):
+            left(mid_all.at[pl.ds(0, K * T - 1)], mid_ss.at[t])
 
 
 def flush(result_v, state_v, result, new_state, sem):
@@ -581,6 +579,8 @@
             V((n, 1, W), F32),
             V(w_gate.shape[::-1], BF16),
             V(w_up.shape[::-1], BF16),
+            V(w_gate.shape, BF16),
+            V(w_up.shape, BF16),
             V(w_down.shape, BF16),
             V((K, RL, DK), F32),
             V((K, RL, DK), F32),
@@ -597,23 +597,23 @@
             pltpu.SemaphoreType.REGULAR,
             dma,
             dma,
+            dma,
+            dma,
+            dma,
+            dma((T, 2)),
+            dma,
+            dma,
+            dma,
+            dma,
+            dma,
+            dma,
+            dma,
+            dma,
             dma((K,)),
-            dma((K,)),
-            dma((4, K)),
-            dma((T, 4, K)),
-            dma((2, K)),
-            dma,
-            dma,
-            dma,
-            dma,
-            dma,
-            dma,
-            dma((K,)),
-            dma((K,)),
-            dma((K, T, T)),
+            dma((T,)),
             dma((K, T)),
-            dma((K, T)),
-            dma((K, T)),
+            dma,
+            dma,
         ],
         compiler_params=pltpu.CompilerParams(
             collective_id=0, has_side_effects=True, vmem_limit_bytes=60 * 1024 * 1024

time: 22.8 us -> 21.9 us (0.961)
  Pallas kernels: 22 us -> 21.1 us
    pallas_call x1, Pallas kernels: 21 us -> 20.1 us  [body(): pl.pallas_call(functools.partial(kernel, K, T), out_shape=(pltpu.VMEM((R,...]
where the time goes in v5:
time: 21.9 us; the launch traced here: 21.7 us
  Pallas kernels  21.1 us (96%)
  between operations  0.64 us (3%)
    pallas_call x1, Pallas kernels, body(): pl.pallas_call(functools.partial(kernel, K, T), out_shape=(pltpu.VMEM((R,...  20.1 us
    pallas_call x1, Pallas kernels, body(): pl.pallas_call(flush, out_shape=(jax.ShapeDtypeStruct((R, W), BF16), jax....  0.99 us

profile of v5, /device:TPU:0, one launch (start us, length us, event | category | flops | bytes accessed | tf_op | source)
XLA Modules:
  0.0 21.7 jit_solution(10260679783387874662)
XLA Ops:
  0.6 20.1 %shard_map.149 = (bf16[8,256]{1,0:T(8,128)(2,1)S(1)}, f32[2,8,128,128]{3,2,1,0:T(8,128)S(1)}) custom-call(bf16[8,256]{1,0:T(8,128)(2,1)} %tokens.1, f32[2,8,128,128]{3,2,1,0:T(8,128)} %past.1, f32[2,1,256]{2,1,0:T(1,128)} %bitcast.10, bf16[512,1024]{1,0:T(8,128)(2,1)} %w_query.1, bf16[512,1024]{1,0:T(8,128)(2,1)} %w_forget.1, bf16[512,1024]{1,0:T(8,128)(2,1)} %w_value.1, ...), custom_call_target="tpu_custom_call" | custom-call | tf_op jit(solution)/shard_map/pallas_call | solution.py:563
  20.7 1.0 %shard_map.150 = (bf16[8,256]{1,0:T(8,128)(2,1)}, f32[2,8,128,128]{3,2,1,0:T(8,128)}) custom-call(bf16[8,256]{1,0:T(8,128)(2,1)S(1)} %get-tuple-element.4.result_v, f32[2,8,128,128]{3,2,1,0:T(8,128)S(1)} %get-tuple-element.5.state_v), custom_call_target="tpu_custom_call" | custom-call | tf_op jit(solution)/shard_map/pallas_call | solution.py:622

commit v6 on v5

--- a/solution.py
+++ b/solution.py
@@ -215,29 +215,28 @@
         for k in range(K):
             part_send[i, k] = part[i, k * RL : (k + 1) * RL].reshape(RL * H, DK).astype(BF16)
 
-    def scatter(i):
+    def scatter(*which):
         for j in hops[::-1]:
             k = hop(j)
-            send(
-                part_send.at[i, k],
-                part_recv.at[tp, i, kv],
+            for i in which:
+                send(
+                    part_send.at[i, k],
+                    part_recv.at[tp, i, kv],
+                    part_ss,
+                    part_rs.at[tp, max(i - 1, 0)],
+                    k,
+                    1,
+                )
+        for i in which:
+            own = remote(
+                part_send.at[i, kv],
+                part_recv.at[0, i, kv],
                 part_ss,
-                part_rs.at[tp, i // 2],
-                k,
+                part_rs.at[0, max(i - 1, 0)],
+                kv,
                 1,
             )
-        own = remote(
-            part_send.at[i, kv],
-            part_recv.at[0, i, kv],
-            part_ss,
-            part_rs.at[0, i // 2],
-            kv,
-            1,
-        )
-
-        @pl.when(tp == 0)
-        def _():
-            own.start()
+            pl.when(tp == 0)(own.start)
 
     again = []
     mine = features(tp)
@@ -266,12 +265,11 @@
     for j in hops[::-1]:
         k = hop(j)
         send(sq_send.at[k], sq_recv.at[kv], sq_ss, sq_rs, k, tp)
-    scatter(0)
-    scatter(1)
+    scatter(0, 1)
     push = remote(w_out, wout_v.at[0], wout_ss, wout_rs, kv, 1)
-    c_wgate = load(11, w_gate, wgate_v)
-    c_wup = load(12, w_up, wup_v)
-    c_wdown = load(13, w_down, wdown_v)
+    c_wgate = load(0, w_gate, wgate_v)
+    c_wup = load(1, w_up, wup_v)
+    c_wdown = load(2, w_down, wdown_v)
     totals = []
     for i in range(2, 4):
         c_proj[i].wait()
@@ -288,7 +286,7 @@
                     part_send.at[i, k],
                     part_recv.at[0, i, kv],
                     again_ss,
-                    part_rs.at[0, i // 2],
+                    part_rs.at[0, max(i - 1, 0)],
                     k,
                     0,
                 )
@@ -311,7 +309,7 @@
 
     @pl.when(tp == 1)
     def _():
-        pltpu.make_async_copy(w_out, wout_v.at[1], local_sem.at[10]).start()
+        pltpu.make_async_copy(w_out, wout_v.at[1], local_sem.at[3]).start()
 
     c_floor.wait()
     c_hgain.wait()
@@ -327,10 +325,11 @@
     def own_part(i):
         return part[i, pl.ds(kv * RL, RL)].reshape(RL * H, DK)
 
-    def both(half):
-        pair = pl.ds(2 * half, 2)
-        arrived(part_recv.at[0, pair], part_ss, part_rs.at[0, half])
-        arrived(part_recv.at[1, pair, most], part_ss, part_rs.at[1, half])
+    def both(first, count):
+        which = pl.ds(first, count)
+        group = max(first - 1, 0)
+        arrived(part_recv.at[0, which], part_ss, part_rs.at[0, group])
+        arrived(part_recv.at[1, which, most], part_ss, part_rs.at[1, group])
 
     def summed(u, i, total):
         for j in hops:
@@ -358,11 +357,12 @@
             jnp.sum(activ * (1.0 - forget), axis=1, keepdims=True),
         )
 
-    def gated(u, head_out, gate_pre):
-        normed = head_out * lax.rsqrt(
-            jnp.mean(head_out * head_out, axis=1, keepdims=True) + epsilon
+    def normed(head_out):
+        return (
+            head_out
+            * lax.rsqrt(jnp.mean(head_out * head_out, axis=1, keepdims=True) + epsilon)
+            * hgain_v[...]
         )
-        mix_all[kv, u] = (normed * hgain_v[...] * silu(gate_pre)).astype(BF16)
 
     @pl.when(tp == 0)
     def _():
@@ -371,7 +371,7 @@
 
     @pl.when(tp == 1)
     def _():
-        both(0)
+        both(0, 2)
 
     forget = forget_of(tp, summed(tp, 0, own_part(0)))
     mix_sends = [
@@ -385,9 +385,12 @@
         arrived(round_v.at[0], past_ss, past_rs)
         zero, zero_rest = weighted(0, forget_of(0, total_of(0, 0)), silu(total_of(0, 1)))
         one, one_rest = weighted(1, forget, silu(total_of(1, 1)))
-        both(1)
-        gated(0, zero + total_of(0, 2) * zero_rest, total_of(0, 3))
-        gated(1, one + total_of(1, 2) * one_rest, total_of(1, 3))
+        both(2, 1)
+        zero = normed(zero + total_of(0, 2) * zero_rest)
+        one = normed(one + total_of(1, 2) * one_rest)
+        both(3, 1)
+        mix_all[kv, 0] = (zero * silu(total_of(0, 3))).astype(BF16)
+        mix_all[kv, 1] = (one * silu(total_of(1, 3))).astype(BF16)
         for copy in mix_sends:
             copy.start()
 
@@ -423,13 +426,15 @@
         every_head = jnp.concatenate(
             [mix_f[t, :, h, :].astype(BF16) for t in range(T) for h in range(H)], axis=1
         )
-        pltpu.make_async_copy(w_out, wout_v.at[1], local_sem.at[10]).wait()
+        pltpu.make_async_copy(w_out, wout_v.at[1], local_sem.at[3]).wait()
         arrived(wout_v.at[0], wout_ss, wout_rs)
+        middle = [
+            tok_v[t].astype(F32)
+            + jnp.dot(every_head, wout_v[t], preferred_element_type=F32)
+            for t in range(T)
+        ]
         for t in range(T):
-            middle = tok_v[t].astype(F32) + jnp.dot(
-                every_head, wout_v[t], preferred_element_type=F32
-            )
-            mid_all[kv * T + t] = middle.astype(BF16)
+            mid_all[kv * T + t] = middle[t].astype(BF16)
             for copy in given[t * len(given) // T : (t + 1) * len(given) // T]:
                 copy.start()
 
@@ -466,15 +471,27 @@
     mlp_scale = lax.rsqrt(square / D + epsilon)
     hidden = (silu(gate * mlp_scale) * (upward * mlp_scale)).astype(BF16)
     c_wdown.wait()
-    for dk in hops[::-1] + [0]:
-        k, _ = other(dk, 0)
-        lanes = pl.ds(pl.multiple_of(k * T * W, T * W), T * W)
-        chunk = jnp.dot(hidden, wdown_v[:, lanes], preferred_element_type=F32).astype(BF16)
-        for t in range(T):
-            term_send[k * T + t] = chunk[:, t * W : (t + 1) * W]
-        for dt in range(0 if dk else 1, T):
-            _, t = other(dk, dt)
-            send(term_send.at[k * T + t], term_recv.at[me], term_ss, term_rs, k, t)
+    span = 1 if W % 128 == 0 else T
+    last = None
+
+    def give(j, first, chunk):
+        for t in range(first, first + span):
+            slot = hop(j) * T + t
+            term_send[slot] = chunk[:, (t - first) * W : (t - first + 1) * W].astype(BF16)
+            copy = remote(term_send.at[slot], term_recv.at[me], term_ss, term_rs, hop(j), t)
+            if j:
+                copy.start()
+            else:
+                pl.when(tp != t)(copy.start)
+
+    for j in hops[::-1] + [0]:
+        for first in range(0, T, span):
+            lanes = pl.ds(pl.multiple_of((hop(j) * T + first) * W, span * W), span * W)
+            chunk = jnp.dot(hidden, wdown_v[:, lanes], preferred_element_type=F32)
+            if last is not None:
+                give(*last)
+            last = (j, first, chunk)
+    give(*last)
     value = summed(tp, 2, own_part(2))
     columns = forget.T
     for s in range(RL):
@@ -484,28 +501,29 @@
             new_state[s, h] = row + columns[:, i : i + 1] * (past_v[s, h] - row)
 
     total = term_send[me].astype(F32)
+    swap.wait_send()
+    left(sq_send.at[most], sq_ss)
+
+    @pl.when(tp == 0)
+    def _():
+        left(part_send, part_ss)
+        left(part_send.at[pl.ds(0, 2), most], again_ss)
+        for copy in pushes:
+            copy.wait_send()
+
+    @pl.when(tp == 1)
+    def _():
+        left(part_send.at[:, most], part_ss)
+        left(mix_all.at[most], mix_ss)
+        for t in range(T):
+            left(mid_all.at[pl.ds(0, K * T - 1)], mid_ss.at[t])
+
     arrived(term_recv.at[pl.ds(0, K * T - 1)], term_ss, term_rs)
     for dk, dt in near:
         k, t = source(dk, dt)
         total = total + term_recv[k * T + t].astype(F32)
     result[...] = (mid_all[me].astype(F32) + total).astype(BF16)
-    swap.wait_send()
-    left(sq_send.at[most], sq_ss)
     left(term_send.at[pl.ds(0, K * T - 1)], term_ss)
-
-    @pl.when(tp == 0)
-    def _():
-        left(part_send, part_ss)
-        left(part_send.at[pl.ds(0, 2), most], again_ss)
-        for copy in pushes:
-            copy.wait_send()
-
-    @pl.when(tp == 1)
-    def _():
-        left(part_send.at[:, most], part_ss)
-        left(mix_all.at[most], mix_ss)
-        for t in range(T):
-            left(mid_all.at[pl.ds(0, K * T - 1)], mid_ss.at[t])
 
 
 def flush(result_v, state_v, result, new_state, sem):
@@ -593,14 +611,14 @@
             V((n, R, W), BF16),
             V((n, R, W), BF16),
             V((n, R, W), BF16),
-            dma((14,)),
+            dma((10,)),
             pltpu.SemaphoreType.REGULAR,
             dma,
             dma,
             dma,
             dma,
             dma,
-            dma((T, 2)),
+            dma((T, 3)),
             dma,
             dma,
             dma,

time: 21.9 us -> 21.7 us (level)
  no operation moved by 1% of the time
where the time goes in v6:
time: 21.7 us; the launch traced here: 21.6 us
  Pallas kernels  20.9 us (96%)
  between operations  0.64 us (3%)
    pallas_call x1, Pallas kernels, body(): pl.pallas_call(functools.partial(kernel, K, T), out_shape=(pltpu.VMEM((R,...  19.9 us
    pallas_call x1, Pallas kernels, body(): pl.pallas_call(flush, out_shape=(jax.ShapeDtypeStruct((R, W), BF16), jax....  0.99 us

profile of v6, /device:TPU:0, one launch (start us, length us, event | category | flops | bytes accessed | tf_op | source)
XLA Modules:
  0.0 21.6 jit_solution(4825252678160045382)
XLA Ops:
  0.6 19.9 %shard_map.149 = (bf16[8,256]{1,0:T(8,128)(2,1)S(1)}, f32[2,8,128,128]{3,2,1,0:T(8,128)S(1)}) custom-call(bf16[8,256]{1,0:T(8,128)(2,1)} %tokens.1, f32[2,8,128,128]{3,2,1,0:T(8,128)} %past.1, f32[2,1,256]{2,1,0:T(1,128)} %bitcast.10, bf16[512,1024]{1,0:T(8,128)(2,1)} %w_query.1, bf16[512,1024]{1,0:T(8,128)(2,1)} %w_forget.1, bf16[512,1024]{1,0:T(8,128)(2,1)} %w_value.1, ...), custom_call_target="tpu_custom_call" | custom-call | tf_op jit(solution)/shard_map/pallas_call | solution.py:581
  20.6 1.0 %shard_map.150 = (bf16[8,256]{1,0:T(8,128)(2,1)}, f32[2,8,128,128]{3,2,1,0:T(8,128)}) custom-call(bf16[8,256]{1,0:T(8,128)(2,1)S(1)} %get-tuple-element.4.result_v, f32[2,8,128,128]{3,2,1,0:T(8,128)S(1)} %get-tuple-element.5.state_v), custom_call_target="tpu_custom_call" | custom-call | tf_op jit(solution)/shard_map/pallas_call | solution.py:640

commit v7 on v6

--- a/solution.py
+++ b/solution.py
@@ -353,9 +353,14 @@
             [jnp.where(owner == i, weight, 0.0).astype(BF16) for i in range(RL * H)], axis=1
         )
         return (
-            jnp.dot(left, round_v[u], preferred_element_type=F32),
+            halves(left, round_v.at[u]),
             jnp.sum(activ * (1.0 - forget), axis=1, keepdims=True),
         )
+
+    def halves(a, b):
+        cut = b.shape[0] // 2
+        first = jnp.dot(a[:, :cut], b[:cut, :], preferred_element_type=F32)
+        return first + jnp.dot(a[:, cut:], b[cut:, :], preferred_element_type=F32)
 
     def normed(head_out):
         return (
@@ -430,7 +435,7 @@
         arrived(wout_v.at[0], wout_ss, wout_rs)
         middle = [
             tok_v[t].astype(F32)
-            + jnp.dot(every_head, wout_v[t], preferred_element_type=F32)
+            + halves(every_head, wout_v.at[t])
             for t in range(T)
         ]
         for t in range(T):

time: 21.7 us -> 21.6 us (level)
  no operation moved by 1% of the time
where the time goes in v7:
time: 21.6 us; the launch traced here: 21.4 us
  Pallas kernels  20.7 us (96%)
  between operations  0.64 us (3%)
    pallas_call x1, Pallas kernels, body(): pl.pallas_call(functools.partial(kernel, K, T), out_shape=(pltpu.VMEM((R,...  19.7 us
    pallas_call x1, Pallas kernels, body(): pl.pallas_call(flush, out_shape=(jax.ShapeDtypeStruct((R, W), BF16), jax....  0.99 us

profile of v7, /device:TPU:0, one launch (start us, length us, event | category | flops | bytes accessed | tf_op | source)
XLA Modules:
  0.0 21.4 jit_solution(4587939297073994068)
XLA Ops:
  0.6 19.7 %shard_map.149 = (bf16[8,256]{1,0:T(8,128)(2,1)S(1)}, f32[2,8,128,128]{3,2,1,0:T(8,128)S(1)}) custom-call(bf16[8,256]{1,0:T(8,128)(2,1)} %tokens.1, f32[2,8,128,128]{3,2,1,0:T(8,128)} %past.1, f32[2,1,256]{2,1,0:T(1,128)} %bitcast.10, bf16[512,1024]{1,0:T(8,128)(2,1)} %w_query.1, bf16[512,1024]{1,0:T(8,128)(2,1)} %w_forget.1, bf16[512,1024]{1,0:T(8,128)(2,1)} %w_value.1, ...), custom_call_target="tpu_custom_call" | custom-call | tf_op jit(solution)/shard_map/pallas_call | solution.py:586
  20.4 1.0 %shard_map.150 = (bf16[8,256]{1,0:T(8,128)(2,1)}, f32[2,8,128,128]{3,2,1,0:T(8,128)}) custom-call(bf16[8,256]{1,0:T(8,128)(2,1)S(1)} %get-tuple-element.4.result_v, f32[2,8,128,128]{3,2,1,0:T(8,128)S(1)} %get-tuple-element.5.state_v), custom_call_target="tpu_custom_call" | custom-call | tf_op jit(solution)/shard_map/pallas_call | solution.py:645

commit v8 on v7

--- a/solution.py
+++ b/solution.py
@@ -81,9 +81,7 @@
     wout_rs,
     mix_ss,
     mix_rs,
-    mid_ss,
     mid_rs,
-    term_ss,
     term_rs,
 ):
     R, W = tokens.shape
@@ -405,6 +403,19 @@
         for c in range(0, D, step):
             dst[c : c + step, :] = src[:, c : c + step].T
 
+    swap.wait_send()
+    left(sq_send.at[most], sq_ss)
+
+    @pl.when(tp == 0)
+    def _():
+        left(part_send, part_ss)
+
+    @pl.when(tp == 1)
+    def _():
+        left(part_send.at[:, most], part_ss)
+
+    term_ss = tok_ss
+    mid_ss = (sq_ss, part_ss)
     turn(c_wgate, wgate_v, gatet_v)
     turn(c_wup, wup_v, upt_v)
 
@@ -417,7 +428,7 @@
         for j in hops[::-1] + [0]:
             for peer in range(1 if j == 0 else T):
                 given.append(
-                    remote(slot, slot, mid_ss.at[t], mid_rs.at[kv, t], hop(j), peer)
+                    remote(slot, slot, mid_ss[t], mid_rs.at[kv, t], hop(j), peer)
                 )
 
     @pl.when(tp == 1)
@@ -454,12 +465,12 @@
         k = hop(group[0][0])
         for j, t in group:
             if j:
-                arrived(mid_all.at[k * T + t], mid_ss.at[t], mid_rs.at[k, t])
+                arrived(mid_all.at[k * T + t], mid_ss[t], mid_rs.at[k, t])
             else:
 
                 @pl.when(tp == 0)
                 def _(t=t):
-                    arrived(mid_all.at[kv * T + t], mid_ss.at[t], mid_rs.at[kv, t])
+                    arrived(mid_all.at[kv * T + t], mid_ss[t], mid_rs.at[kv, t])
 
         j = k * T + group[0][1]
         blocks = []
@@ -492,7 +503,12 @@
     for j in hops[::-1] + [0]:
         for first in range(0, T, span):
             lanes = pl.ds(pl.multiple_of((hop(j) * T + first) * W, span * W), span * W)
-            chunk = jnp.dot(hidden, wdown_v[:, lanes], preferred_element_type=F32)
+            cut = hidden.shape[1] // 256 // 2 * 256
+            chunk = jnp.dot(hidden[:, cut:], wdown_v[cut:, lanes], preferred_element_type=F32)
+            if cut:
+                chunk = chunk + jnp.dot(
+                    hidden[:, :cut], wdown_v[:cut, lanes], preferred_element_type=F32
+                )
             if last is not None:
                 give(*last)
             last = (j, first, chunk)
@@ -506,22 +522,18 @@
             new_state[s, h] = row + columns[:, i : i + 1] * (past_v[s, h] - row)
 
     total = term_send[me].astype(F32)
-    swap.wait_send()
-    left(sq_send.at[most], sq_ss)
 
     @pl.when(tp == 0)
     def _():
-        left(part_send, part_ss)
         left(part_send.at[pl.ds(0, 2), most], again_ss)
         for copy in pushes:
             copy.wait_send()
 
     @pl.when(tp == 1)
     def _():
-        left(part_send.at[:, most], part_ss)
         left(mix_all.at[most], mix_ss)
         for t in range(T):
-            left(mid_all.at[pl.ds(0, K * T - 1)], mid_ss.at[t])
+            left(mid_all.at[pl.ds(0, K * T - 1)], mid_ss[t])
 
     arrived(term_recv.at[pl.ds(0, K * T - 1)], term_ss, term_rs)
     for dk, dt in near:
@@ -633,9 +645,7 @@
             dma,
             dma,
             dma((K,)),
-            dma((T,)),
             dma((K, T)),
-            dma,
             dma,
         ],
         compiler_params=pltpu.CompilerParams(

time: 21.6 us -> 21.6 us (level)
  no operation moved by 1% of the time
where the time goes in v8:
time: 21.6 us; the launch traced here: 21.4 us
  Pallas kernels  20.7 us (96%)
  between operations  0.64 us (3%)
    pallas_call x1, Pallas kernels, body(): pl.pallas_call(functools.partial(kernel, K, T), out_shape=(pltpu.VMEM((R,...  19.7 us
    pallas_call x1, Pallas kernels, body(): pl.pallas_call(flush, out_shape=(jax.ShapeDtypeStruct((R, W), BF16), jax....  0.99 us

profile of v8, /device:TPU:0, one launch (start us, length us, event | category | flops | bytes accessed | tf_op | source)
XLA Modules:
  0.0 21.4 jit_solution(17986869340853221517)
XLA Ops:
  0.6 19.7 %shard_map.149 = (bf16[8,256]{1,0:T(8,128)(2,1)S(1)}, f32[2,8,128,128]{3,2,1,0:T(8,128)S(1)}) custom-call(bf16[8,256]{1,0:T(8,128)(2,1)} %tokens.1, f32[2,8,128,128]{3,2,1,0:T(8,128)} %past.1, f32[2,1,256]{2,1,0:T(1,128)} %bitcast.10, bf16[512,1024]{1,0:T(8,128)(2,1)} %w_query.1, bf16[512,1024]{1,0:T(8,128)(2,1)} %w_forget.1, bf16[512,1024]{1,0:T(8,128)(2,1)} %w_value.1, ...), custom_call_target="tpu_custom_call" | custom-call | tf_op jit(solution)/shard_map/pallas_call | solution.py:598
  20.4 1.0 %shard_map.150 = (bf16[8,256]{1,0:T(8,128)(2,1)}, f32[2,8,128,128]{3,2,1,0:T(8,128)}) custom-call(bf16[8,256]{1,0:T(8,128)(2,1)S(1)} %get-tuple-element.4.result_v, f32[2,8,128,128]{3,2,1,0:T(8,128)S(1)} %get-tuple-element.5.state_v), custom_call_target="tpu_custom_call" | custom-call | tf_op jit(solution)/shard_map/pallas_call | solution.py:655

commit v9 on v7

--- a/solution.py
+++ b/solution.py
@@ -406,7 +406,7 @@
             dst[c : c + step, :] = src[:, c : c + step].T
 
     turn(c_wgate, wgate_v, gatet_v)
-    turn(c_wup, wup_v, upt_v)
+    c_wup.wait()
 
     def spread(t, k):
         mix_f[t, pl.ds(k * RL, RL)] = mix_all[k, t].astype(F32).reshape(RL, H, DV)
@@ -471,7 +471,7 @@
         width = len(group) * W
         lanes = pl.ds(pl.multiple_of(j * W, width), width)
         g = jnp.dot(block, gatet_v[lanes, :], preferred_element_type=F32)
-        u = jnp.dot(block, upt_v[lanes, :], preferred_element_type=F32)
+        u = lax.dot_general(block, wup_v[:, lanes], (((1,), (1,)), ((), ())), preferred_element_type=F32)
         gate, upward = (g, u) if gate is None else (gate + g, upward + u)
     mlp_scale = lax.rsqrt(square / D + epsilon)
     hidden = (silu(gate * mlp_scale) * (upward * mlp_scale)).astype(BF16)

time: 21.6 us -> 21.6 us (level)
  no operation moved by 1% of the time
where the time goes in v9:
time: 21.6 us; the launch traced here: 21.4 us
  Pallas kernels  20.8 us (96%)
  between operations  0.64 us (3%)
    pallas_call x1, Pallas kernels, body(): pl.pallas_call(functools.partial(kernel, K, T), out_shape=(pltpu.VMEM((R,...  19.8 us
    pallas_call x1, Pallas kernels, body(): pl.pallas_call(flush, out_shape=(jax.ShapeDtypeStruct((R, W), BF16), jax....  0.99 us

profile of v9, /device:TPU:0, one launch (start us, length us, event | category | flops | bytes accessed | tf_op | source)
XLA Modules:
  0.0 21.4 jit_solution(1254078470154696672)
XLA Ops:
  0.6 19.8 %shard_map.149 = (bf16[8,256]{1,0:T(8,128)(2,1)S(1)}, f32[2,8,128,128]{3,2,1,0:T(8,128)S(1)}) custom-call(bf16[8,256]{1,0:T(8,128)(2,1)} %tokens.1, f32[2,8,128,128]{3,2,1,0:T(8,128)} %past.1, f32[2,1,256]{2,1,0:T(1,128)} %bitcast.10, bf16[512,1024]{1,0:T(8,128)(2,1)} %w_query.1, bf16[512,1024]{1,0:T(8,128)(2,1)} %w_forget.1, bf16[512,1024]{1,0:T(8,128)(2,1)} %w_value.1, ...), custom_call_target="tpu_custom_call" | custom-call | tf_op jit(solution)/shard_map/pallas_call | solution.py:586
  20.4 1.0 %shard_map.150 = (bf16[8,256]{1,0:T(8,128)(2,1)}, f32[2,8,128,128]{3,2,1,0:T(8,128)}) custom-call(bf16[8,256]{1,0:T(8,128)(2,1)S(1)} %get-tuple-element.4.result_v, f32[2,8,128,128]{3,2,1,0:T(8,128)S(1)} %get-tuple-element.5.state_v), custom_call_target="tpu_custom_call" | custom-call | tf_op jit(solution)/shard_map/pallas_call | solution.py:645
